TPU v7x, 256 devices: a whole 4x4x8 slice. The times are simulated.
256 devices in a mesh: ep: 32 (over z, x), tp: 8 (over y, core).
Axes of the slice: x: 4, y: 4, z: 8, core: 2. Of those that a mesh axis runs over, the one named last changes fastest.
Arguments:
- queries: bfloat16 [8192, 2048], P('ep', 'tp'), may hold values from -9 to 9
- keys: bfloat16 [8192, 2048], P('ep', 'tp'), may hold values from -9 to 9
- values: bfloat16 [8192, 2048], P('ep', 'tp'), may hold values from -6 to 6
- lambdas: float32 [16], P('tp'), may hold values from 0.3 to 0.8
- head_gain: float32 [128], replicated, may hold values from 0.1 to 1.9
- moe_input: bfloat16 [32768, 2048], P('ep'), may hold values from -6 to 6
- ffn_gain: float32 [2048], replicated, may hold values from 0.1 to 1.9
- group_router: bfloat16 [2048, 4], replicated, may hold values from -0.125 to 0.125
- expert_router: bfloat16 [2048, 32], replicated, may hold values from -0.125 to 0.125
- routes: int32 [32768, 2], P('ep'), may hold values from 0 to 31, as said below
- w_gate: bfloat16 [32, 2048, 1024], P('ep', None, 'tp'), may hold values from -0.125 to 0.125
- w_up: bfloat16 [32, 2048, 1024], P('ep', None, 'tp'), may hold values from -0.125 to 0.125
- w_down: bfloat16 [32, 1024, 2048], P('ep', 'tp'), may hold values from -0.1875 to 0.1875
Outputs:
- attn_out: bfloat16 [8192, 2048], P('ep', 'tp')
- moe_out: bfloat16 [32768, 2048], P(('ep', 'tp'))
Inputs may be any that keep to these rules, and one draw needn't show every extreme that they name: `routes`: in each aligned block of 128 rows (the rows of one device) every expert is named by exactly 8 rows and every group by the same number of rows; a row's two experts differ and lie in one group of 8 consecutive expert numbers.
All inputs are finite; a program needn't handle non-finite values.
Results may differ from a plain program's by a relative error of at most 0.015.
Values may be sent and summed in bfloat16 or wider, within the bound.
No kernel may reach another device: no remote copies, remote signals or barrier semaphores. Data moves between devices by JAX's collectives and lax.ppermute only.
A program may use at most 128 MiB of HBM per device.

v0:
```python
import math

import jax
import jax.numpy as jnp
from jax import lax
from jax.sharding import Mesh
from jax.sharding import PartitionSpec as P

EP = ("ep_0", "ep_1")
EP_TP = ("ep_0", "ep_1", "tp")


norm_eps = 1e-06
masked_score = -1e30


def gathered_by_axis(array, axes, dim):
    for axis in reversed(axes):
        array = lax.all_gather(array, axis, axis=dim, tiled=True)
    return array


def in_one_piece(arrays, axis, dim, along):
    both = jnp.concatenate(arrays, axis=along)
    whole, at, outs = (lax.all_gather(both, axis, axis=dim, tiled=True), 0, [])
    for a in arrays:
        outs.append(lax.slice_in_dim(whole, at, at + a.shape[along], axis=along))
        at += a.shape[along]
    return tuple(outs)


def rows_first(arrays, axis, dims):
    turned = [jnp.moveaxis(a, dim, 0) for a, dim in zip(arrays, dims)]
    widths = [t[0].size for t in turned]
    both = jnp.concatenate([t.reshape(-1, w) for t, w in zip(turned, widths)], axis=1)
    whole = lax.all_gather(both, axis, axis=0, tiled=True)
    parts = jnp.split(whole, [sum(widths[:k]) for k in range(1, len(widths))], axis=1)
    return tuple(
        (
            jnp.moveaxis(b.reshape(-1, *t.shape[1:]), 0, dim)
            for b, t, dim in zip(parts, turned, dims)
        )
    )


def cut_along(array, dim, size):
    before, after = (array.shape[:dim], array.shape[dim + 1 :])
    return jnp.moveaxis(array.reshape(*before, size, -1, *after), dim, 0)


def piece_ends(length, count):
    unit = 8 if length >= 8 * count else 1
    return [length // unit * k // count * unit for k in range(1, count)]


def laid_out(parts, dim):
    parts = jnp.moveaxis(parts, 0, dim)
    shape = parts.shape
    return parts.reshape(*shape[:dim], shape[dim] * shape[dim + 1], *shape[dim + 2 :])


def several_exchanges(array, axis, pieces, split_dim, concat_dim):
    parts = cut_along(array, split_dim, lax.axis_size(axis))
    cut = max(range(1, max(2, parts.ndim - 1)), key=lambda d: parts.shape[d])
    outs = []
    for slab in jnp.split(parts, piece_ends(parts.shape[cut], pieces), axis=cut):
        if slab.size:
            outs.append(lax.all_to_all(slab, axis, split_axis=0, concat_axis=0, tiled=True))
    return laid_out(jnp.concatenate(outs, axis=cut), concat_dim)


def rms_scaled(rows, gain):
    widened = rows.astype(jnp.float32)
    return (
        widened * lax.rsqrt(jnp.mean(widened * widened, axis=-1, keepdims=True) + norm_eps) * gain
    )


def score_block(query_heads, key_rows, score_scale):
    key_heads = key_rows.reshape(key_rows.shape[0], query_heads.shape[1], 2, query_heads.shape[3])
    return (
        jnp.einsum("qhmd,khmd->hmqk", query_heads, key_heads, preferred_element_type=jnp.float32)
        * score_scale
    )


def route_gates(normed, own_routes, group_router, expert_router):
    group_count = group_router.shape[1]
    expert_count = expert_router.shape[1]
    group_logits = jnp.dot(normed, group_router, preferred_element_type=jnp.float32)
    expert_logits = jnp.dot(normed, expert_router, preferred_element_type=jnp.float32)
    chosen = own_routes[:, 0] // (expert_count // group_count)
    group_mask = jnp.arange(group_count, dtype=jnp.int32)[None, :] == chosen[:, None]
    own_logit = jnp.sum(jnp.where(group_mask, group_logits, 0.0), axis=-1, keepdims=True)
    group_share = 1.0 / jnp.sum(jnp.exp(group_logits - own_logit), axis=-1)
    expert_mask = jnp.arange(expert_count, dtype=jnp.int32)[None, None, :] == own_routes[:, :, None]
    picked = jnp.sum(jnp.where(expert_mask, expert_logits[:, None, :], 0.0), axis=-1)
    return group_share[:, None] * jax.nn.sigmoid(picked - picked[:, ::-1])


def slot_places(own_routes, expert_count, capacity):
    flat_routes = own_routes.reshape(-1)
    one_hot = (flat_routes[:, None] == jnp.arange(expert_count, dtype=jnp.int32)[None, :]).astype(
        jnp.int32
    )
    earlier = jnp.cumsum(one_hot, axis=0) - one_hot
    return flat_routes * capacity + jnp.sum(earlier * one_hot, axis=1)


def dispatch_rows(normed_rows, own_routes, expert_count, capacity):
    places = slot_places(own_routes, expert_count, capacity)
    owners = jnp.arange(places.shape[0], dtype=jnp.int32) // 2
    holder = jnp.zeros((expert_count * capacity,), jnp.int32).at[places].set(owners)
    return normed_rows[holder].reshape(expert_count, capacity, normed_rows.shape[1])


def local(
    queries,
    keys,
    values,
    lambdas,
    head_gain,
    moe_input,
    ffn_gain,
    group_router,
    expert_router,
    routes,
    w_gate,
    w_up,
    w_down,
):
    query_count = queries.shape[0]
    heads_here = lambdas.shape[0]
    value_width = values.shape[1] // heads_here
    qk_width = queries.shape[1] // (2 * heads_here)
    query_heads = queries.reshape(query_count, heads_here, 2, qk_width)
    score_scale = qk_width ** (-0.5)
    query_first = lax.axis_index(EP) * query_count
    query_pos = query_first + jnp.arange(query_count, dtype=jnp.int32)
    query_last = query_first + query_count - 1
    stats_start = (
        jnp.full((heads_here, 2, query_count), masked_score, jnp.float32),
        jnp.zeros((heads_here, 2, query_count), jnp.float32),
    )
    key_shard = gathered_by_axis(keys, EP, 0)
    block_rows = math.gcd(key_shard.shape[0], 512)

    def stats_sweep_step(number, current):
        offset = number * block_rows

        def stats_compute(running):
            maxima, totals = running
            key_pos = offset + jnp.arange(block_rows, dtype=jnp.int32)
            allowed = key_pos[None, :] <= query_pos[:, None]
            key_block = lax.dynamic_slice_in_dim(key_shard, offset, block_rows, 0)
            scores = jnp.where(
                allowed, score_block(query_heads, key_block, score_scale), masked_score
            )
            new_max = jnp.maximum(maxima, jnp.max(scores, axis=-1))
            weights = jnp.where(allowed, jnp.exp(scores - new_max[..., None]), 0.0)
            return (new_max, totals * jnp.exp(maxima - new_max) + jnp.sum(weights, axis=-1))

        return lax.cond(offset <= query_last, stats_compute, lambda running: running, current)

    maxima, totals = lax.fori_loop(
        0, key_shard.shape[0] // block_rows, stats_sweep_step, stats_start
    )
    value_key_shard, value_shard = in_one_piece((keys, values), EP, 0, 1)
    value_block_rows = math.gcd(value_key_shard.shape[0], 512)

    def value_sweep_step(number, current):
        offset = number * value_block_rows

        def value_compute(running):
            key_pos = offset + jnp.arange(value_block_rows, dtype=jnp.int32)
            allowed = key_pos[None, :] <= query_pos[:, None]
            key_block = lax.dynamic_slice_in_dim(value_key_shard, offset, value_block_rows, 0)
            scores = score_block(query_heads, key_block, score_scale)
            shares = (
                jnp.where(allowed, jnp.exp(scores - maxima[..., None]), 0.0) / totals[..., None]
            )
            mixed = (shares[:, 0] - lambdas[:, None, None] * shares[:, 1]).astype(jnp.bfloat16)
            value_rows = lax.dynamic_slice_in_dim(value_shard, offset, value_block_rows, 0).reshape(
                value_block_rows, heads_here, value_width
            )
            return running + jnp.einsum(
                "hqk,khd->hqd", mixed, value_rows, preferred_element_type=jnp.float32
            )

        return lax.cond(offset <= query_last, value_compute, lambda running: running, current)

    heads_out = lax.fori_loop(
        0,
        value_key_shard.shape[0] // value_block_rows,
        value_sweep_step,
        jnp.zeros((heads_here, query_count, value_width), jnp.float32),
    )
    attn_out = rms_scaled(heads_out, head_gain).astype(jnp.bfloat16)
    attn_out = attn_out.transpose(1, 0, 2).reshape(query_count, heads_here * value_width)
    tp_count = lax.axis_size("tp")
    tp_index = lax.axis_index("tp")
    own_count = routes.shape[0] // tp_count
    expert_count = expert_router.shape[1]
    capacity = 2 * own_count // expert_count
    model_width = moe_input.shape[1]
    own_routes = lax.dynamic_slice_in_dim(routes, tp_index * own_count, own_count, 0)
    gate_local = w_gate[0]
    up_local = w_up[0]
    down_local = w_down[0]
    own_input = lax.dynamic_slice_in_dim(moe_input, tp_index * own_count, own_count, 0)
    normed = rms_scaled(own_input, ffn_gain).astype(jnp.bfloat16)
    packed = dispatch_rows(normed, own_routes, expert_count, capacity)
    arrived = lax.all_to_all(packed, EP, split_axis=0, concat_axis=0, tiled=True)
    gate_whole, up_whole, down_whole = rows_first(
        (gate_local, up_local, down_local), "tp", (1, 1, 0)
    )
    arrived_rows = arrived.reshape(-1, model_width)
    gate_part = jnp.dot(arrived_rows, gate_whole, preferred_element_type=jnp.float32)
    up_part = jnp.dot(arrived_rows, up_whole, preferred_element_type=jnp.float32)
    hidden = (jax.nn.silu(gate_part) * up_part).astype(jnp.bfloat16)
    part_width = down_local.shape[0]
    pieces = hidden.reshape(hidden.shape[0], tp_count, part_width)
    down_parts = down_whole.reshape(tp_count, part_width, model_width)
    partial_value = jnp.einsum(
        "nsf,sfd->snd", pieces, down_parts, preferred_element_type=jnp.float32
    ).astype(jnp.bfloat16)
    results = jnp.sum(partial_value.astype(jnp.float32), axis=0).astype(jnp.bfloat16)
    homed = several_exchanges(results.reshape(expert_count, capacity, model_width), EP, 2, 0, 0)
    places = slot_places(own_routes, expert_count, capacity)
    returned = homed.reshape(expert_count * capacity, model_width)[places].reshape(
        own_count, 2, model_width
    )
    gates = route_gates(normed, own_routes, group_router, expert_router)
    moe_out = jnp.sum(returned.astype(jnp.float32) * gates[..., None], axis=1).astype(jnp.bfloat16)
    return (attn_out, moe_out)


def solution(mesh):
    split = Mesh(mesh.devices.reshape(8, 4, mesh.shape["tp"]), ("ep_0", "ep_1", "tp"))
    placed = (
        P(EP, "tp"),
        P(EP, "tp"),
        P(EP, "tp"),
        P("tp"),
        P(),
        P(EP, None),
        P(),
        P(),
        P(),
        P(EP, None),
        P(EP, None, "tp"),
        P(EP, None, "tp"),
        P(EP, "tp", None),
    )
    return jax.shard_map(
        local, mesh=split, in_specs=placed, out_specs=(P(EP, "tp"), P(EP_TP, None)), check_vma=False
    )
```

profile of v0, /device:TPU:238, one launch (start us, length us, event | category | flops | bytes accessed | tf_op | source)
XLA Modules:
  0.0 315.7 jit_solution(4053415805564961571)
XLA Ops:
  11.4 14.2 %all_gather.13 = bf16[1024,256]{0,1:T(8,128)(2,1)} all-gather(bf16[256,256]{0,1:T(8,128)(2,1)S(1)} %copy.63), channel_id=1, replica_groups=mesh['ep_0'=8,'ep_1'=4,'tp'=8] {'ep_1'}, dimensions={0}, use_global_device_ids=true | all-gather | bytes 655360 | tf_op jit(solution)/shard_map/all_gather | solution.py:19
  35.1 8.3 %all-to-all-start = ((bf16[32,8,2048]{2,1,0:T(8,128)(2,1)}), bf16[32,8,2048]{2,1,0:T(8,128)(2,1)S(1)}, u32[]{:S(2)}, u32[]{:S(2)}) async-start(bf16[32,8,2048]{2,1,0:T(8,128)(2,1)} %bitcast.12), calls=%async_computation | async-start | bytes 2097152 | tf_op jit(solution)/shard_map/all_to_all | solution.py:213
  43.9 37.0 %all-gather.8.cloned.1.call-done = bf16[1024,6144]{1,0:T(8,128)(2,1)} async-done(((bf16[128,6144]{1,0:T(8,128)(2,1)}), bf16[1024,6144]{1,0:T(8,128)(2,1)}) %all-gather.8.cloned.1.call-update) | async-done | bytes 12582928 | tf_op jit(solution)/shard_map/all_gather | solution.py:36
  80.9 3.5 %fusion.13 = f32[256,1024]{1,0:T(8,128)S(1)} fusion(bf16[1024,6144]{1,0:T(8,128)(2,1)} %all-gather.8.cloned.1.call-done, bf16[32,8,2048]{2,1,0:T(8,128)(2,1)S(1)} %all-to-all-done), kind=kOutput, calls=%fused_computation.30 | convolution fusion | flops 1073741824 | bytes 6291456 | tf_op jit(solution)/shard_map/dot_general | solution.py:218
  84.4 3.7 %fusion.21 = bf16[32,8,8,128]{3,2,1,0:T(8,128)(2,1)S(1)} fusion(bf16[1024,6144]{1,0:T(8,128)(2,1)} %all-gather.8.cloned.1.call-done, bf16[32,8,2048]{2,1,0:T(8,128)(2,1)S(1)} %all-to-all-done, f32[256,1024]{1,0:T(8,128)S(1)} %fusion.13), kind=kOutput, calls=%fused_computation.38 | convolution fusion | flops 1075314688 | bytes 6815744 | tf_op jit(solution)/shard_map/dot_general | solution.py:219
  92.0 9.6 %all-to-all-start.1 = ((bf16[32,1,4,2048]{3,2,1,0:T(4,128)(2,1)}), bf16[32,1,4,2048]{3,2,1,0:T(4,128)(2,1)S(1)}, u32[]{:S(2)}, u32[]{:S(2)}) async-start(bf16[32,1,4,2048]{3,2,1,0:T(4,128)(2,1)} %get-tuple-element.462), calls=%async_computation.1 | async-start | bytes 1048576 | tf_op jit(solution)/shard_map/all_to_all | solution.py:68
  102.1 45.6 %all-gather.6.cloned.1.call-done = bf16[8192,256]{0,1:T(8,128)(2,1)} async-done(((bf16[1024,256]{0,1:T(8,128)(2,1)}), bf16[8192,256]{0,1:T(8,128)(2,1)}) %all-gather.6.cloned.1.call-update) | async-done | bytes 4194320 | tf_op jit(solution)/shard_map/all_gather | solution.py:19
  147.7 37.5 %while.33 = (s32[]{:T(128)}, f32[2,2,256]{2,1,0:T(2,128)S(1)}, f32[2,2,256]{2,1,0:T(2,128)S(1)}, s32[]{:T(128)}, bf16[8192,256]{0,1:T(8,128)(2,1)}, /*index=5*/b...) while((s32[]{:T(128)}, f32[2,2,256]{2,1,0:T(2,128)S(1)}, ...), condition=%wide.region_5.6_spmd.clone, body=%wide.region_0.5_spmd.clone.sunk | while | flops 71437056 | bytes 5566725 | solution.py:165
  185.3 7.2 %all-to-all-start.2 = ((bf16[32,1,4,2048]{3,2,1,0:T(4,128)(2,1)}), bf16[32,1,4,2048]{3,2,1,0:T(4,128)(2,1)S(1)}, u32[]{:S(2)}, u32[]{:S(2)}) async-start(bf16[32,1,4,2048]{3,2,1,0:T(4,128)(2,1)} %get-tuple-element.463), calls=%async_computation.2 | async-start | bytes 1048576 | tf_op jit(solution)/shard_map/all_to_all | solution.py:68
  192.4 61.7 %all-gather.4.cloned.1.call-done = bf16[8192,512]{0,1:T(8,128)(2,1)} async-done(((bf16[256,512]{0,1:T(8,128)(2,1)}), bf16[8192,512]{0,1:T(8,128)(2,1)}) %all-gather.4.cloned.1.call-update) | async-done | bytes 8388624 | tf_op jit(solution)/shard_map/all_gather | solution.py:25
  254.1 5.9 %fusion.39 = (bf16[8192,256]{0,1:T(8,128)(2,1)}, bf16[8192,256]{0,1:T(8,128)(2,1)}) fusion(bf16[8192,512]{0,1:T(8,128)(2,1)} %all-gather.4.cloned.1.call-done), kind=kLoop, calls=%fused_computation.87 | loop fusion | bytes 16777216 | tf_op jit(solution)/shard_map/slice | solution.py:27
  260.1 40.9 %while.34 = (s32[]{:T(128)}, f32[2,256,128]{2,1,0:T(8,128)S(1)}, s32[]{:T(128)}, bf16[8192,256]{0,1:T(8,128)(2,1)}, bf16[256,2,2,64]{0,3,2,1:T(8,128)(2,1)S(1)},...) while((s32[]{:T(128)}, f32[2,256,128]{2,1,0:T(8,128)S(1)}, ...), condition=%wide.region_9.10_spmd.clone, body=%wide.region_6.9_spmd.clone.sunk | while | flops 137298688 | bytes 6701341 | solution.py:192
  262.7 2.5 conditional.7
  270.3 2.5 conditional.7
  272.9 2.5 conditional.7
  275.5 2.5 conditional.7
  278.0 2.5 conditional.7
  280.6 2.5 conditional.7
  283.1 2.5 conditional.7
  285.7 2.5 conditional.7
  288.3 2.5 conditional.7
  290.8 2.5 conditional.7
  295.9 2.5 conditional.7
  305.2 3.9 %multiply_reduce_fusion = bf16[128,2048]{1,0:T(8,128)(2,1)} fusion(f32[128,2,2048]{2,1,0:T(2,128)S(1)} %reshape.127, f32[128,2]{1,0:T(8,128)S(1)} %copy.75), kind=kLoop, calls=%fused_computation.32 | loop fusion | flops 786432 | bytes 2622464 | tf_op jit(solution)/shard_map/reduce_sum | solution.py:234
  (371 shorter events, 147.0 us)
Async XLA Ops:
  7.2 36.4 %copy-start = (bf16[2048,32]{0,1:T(8,128)(2,1)S(1)}, bf16[2048,32]{0,1:T(8,128)(2,1)}, u32[]{:S(2)}) copy-start(bf16[2048,32]{0,1:T(8,128)(2,1)} %param.29) | copy-start | bytes 393220
  7.2 2.6 copy-start.1
  7.2 73.7 %all-gather.8.cloned.1.call-start = ((), (), s32[]{:S(2)}) async-start(), calls=%async_computation.5 | async-start | bytes 14155776 | tf_op jit(solution)/shard_map/all_gather | solution.py:36
  9.8 1.4 copy-start.2
  11.2 14.5 %copy-start.3 = (bf16[256,256]{1,0:T(8,128)(2,1)S(1)}, bf16[256,256]{1,0:T(8,128)(2,1)}, u32[]{:S(2)}) copy-start(bf16[256,256]{1,0:T(8,128)(2,1)} %param.23) | copy-start | bytes 393220
  11.2 20.3 %copy-start.7 = (f32[2048]{0:T(1024)S(1)}, f32[2048]{0:T(1024)}, u32[]{:S(2)}) copy-start(f32[2048]{0:T(1024)} %param.27) | copy-start | bytes 24580
  11.2 136.5 %all-gather.6.cloned.1.call-start = ((), (), s32[]{:S(2)}) async-start(), calls=%async_computation.4 | async-start | bytes 4718592 | tf_op jit(solution)/shard_map/all_gather | solution.py:19
  25.6 228.5 %all-gather.4.cloned.1.call-start = ((), (), s32[]{:S(2)}) async-start(), calls=%async_computation.3 | async-start | bytes 8650752 | tf_op jit(solution)/shard_map/all_gather | solution.py:25
  35.1 8.3 %copy-start.4 = (bf16[256,256]{1,0:T(8,128)(2,1)S(1)}, bf16[256,256]{1,0:T(8,128)(2,1)}, u32[]{:S(2)}) copy-start(bf16[256,256]{1,0:T(8,128)(2,1)} %param.21) | copy-start | bytes 393220
  35.1 45.7 %all-to-all-start = ((bf16[32,8,2048]{2,1,0:T(8,128)(2,1)}), bf16[32,8,2048]{2,1,0:T(8,128)(2,1)S(1)}, u32[]{:S(2)}, u32[]{:S(2)}) async-start(bf16[32,8,2048]{2,1,0:T(8,128)(2,1)} %bitcast.12), calls=%async_computation | async-start | bytes 2097152 | tf_op jit(solution)/shard_map/all_to_all | solution.py:213
  84.3 3.7 %slice-start = ((bf16[1024,6144]{1,0:T(8,128)(2,1)}), bf16[1024,2048]{1,0:T(8,128)(2,1)S(1)}, s32[]{:S(2)}) async-start(bf16[1024,6144]{1,0:T(8,128)(2,1)} %all-gather.8.cloned.1.call-done), calls=%async_computation.6 | async-start | bytes 8388608 | tf_op jit(solution)/shard_map/split | solution.py:37
  90.4 11.2 %copy-start.5 = (bf16[2048,4]{0,1:T(4,128)(2,1)S(1)}, bf16[2048,4]{0,1:T(4,128)(2,1)}, u32[]{:S(2)}) copy-start(bf16[2048,4]{0,1:T(4,128)(2,1)} %param.28) | copy-start | bytes 49156
  92.0 93.3 %all-to-all-start.1 = ((bf16[32,1,4,2048]{3,2,1,0:T(4,128)(2,1)}), bf16[32,1,4,2048]{3,2,1,0:T(4,128)(2,1)S(1)}, u32[]{:S(2)}, u32[]{:S(2)}) async-start(bf16[32,1,4,2048]{3,2,1,0:T(4,128)(2,1)} %get-tuple-element.462), calls=%async_computation.1 | async-start | bytes 1048576 | tf_op jit(solution)/shard_map/all_to_all | solution.py:68
  185.3 116.7 %all-to-all-start.2 = ((bf16[32,1,4,2048]{3,2,1,0:T(4,128)(2,1)}), bf16[32,1,4,2048]{3,2,1,0:T(4,128)(2,1)S(1)}, u32[]{:S(2)}, u32[]{:S(2)}) async-start(bf16[32,1,4,2048]{3,2,1,0:T(4,128)(2,1)} %get-tuple-element.463), calls=%async_computation.2 | async-start | bytes 1048576 | tf_op jit(solution)/shard_map/all_to_all | solution.py:68
  192.4 67.6 %copy-start.6 = (f32[2]{0:T(128)S(1)}, f32[2]{0:T(128)}, u32[]{:S(2)}) copy-start(f32[2]{0:T(128)} %param.24) | copy-start | bytes 28
  260.1 41.1 %copy-start.8 = (f32[128]{0:T(128)S(1)}, f32[128]{0:T(128)}, u32[]{:S(2)}) copy-start(f32[128]{0:T(128)} %param.25) | copy-start | bytes 1540
Sparse Core Ops, SparseCore 0:
  11.3 69.4 all-gather.7
  82.7 65.0 all-gather.5
  150.2 103.8 all-gather.3
where the time goes:
time: 317 us; the launch traced here: 316 us
  waiting for transfers between devices  144 us (45%)
  local copies, waits for them, and re-layouts  50.8 us (16%)
  matrix products  38.5 us (12%)
  starting transfers between devices  25.2 us (8%)
  other arithmetic  25.1 us (8%)
  blocking collectives  14.2 us (4%)
  between operations  14.1 us (4%)
  loops' own time  3.37 us (1%)
    all_gather x1, waiting for transfers between devices, in_one_piece(): whole, at, outs = (lax.all_gather(both, axis, axis=dim, tiled=True), 0, [])  61.7 us
    all_gather x1, waiting for transfers between devices, gathered_by_axis(): array = lax.all_gather(array, axis, axis=dim, tiled=True)  45.6 us
    all_gather x1, waiting for transfers between devices, rows_first(): whole = lax.all_gather(both, axis, axis=0, tiled=True)  37 us
    dot_general x32, matrix products, score_block(): jnp.einsum('qhmd,khmd->hmqk', query_heads, key_heads, preferred_element_t...  20.5 us
    dynamic_slice x16, local copies, waits for them, and re-layouts, value_compute(): lax.dynamic_slice_in_dim(value_shard, offset, value_block_rows, 0)  17.2 us
    all_to_all x2, starting transfers between devices, several_exchanges(): lax.all_to_all(slab, axis, split_axis=0, concat_axis=0, tiled=True)  16.7 us
    dynamic_slice x16, local copies, waits for them, and re-layouts, stats_compute(): key_block = lax.dynamic_slice_in_dim(key_shard, offset, block_rows, 0)  15.6 us
    all_gather x1, blocking collectives, gathered_by_axis(): array = lax.all_gather(array, axis, axis=dim, tiled=True)  14.2 us
  transfers between devices with their start and end apart: 6, of which 3 were waited for; matrix products, arithmetic and copies ran while one was open for 33% of the time, Pallas kernels for 0%

commit v1 on v0

v1 whole, which is shorter than its diff:
```python
import functools
import math

import jax
import jax.numpy as jnp
from jax import lax
from jax.experimental import pallas as pl
from jax.experimental.pallas import tpu as pltpu
from jax.sharding import Mesh
from jax.sharding import PartitionSpec as P


EP = ("z", "x")
EP_TP = ("z", "x", "y", "c")
TP = ("y", "c")

norm_eps = 1e-06
masked_score = -1e30
VMEM_LIMIT = 56 * 1024 * 1024
F32 = jnp.float32
BF16 = jnp.bfloat16


def shifted(array, axis, by):
    n = lax.axis_size(axis)
    return lax.ppermute(array, axis, [(i, (i + by) % n) for i in range(n)])


def whole(shape):
    return pl.BlockSpec(shape, lambda *_: (0,) * len(shape))


def slot_masks(routes_t, expert_count, capacity):
    tokens = routes_t.shape[1]
    experts = lax.broadcasted_iota(jnp.int32, (expert_count, tokens), 0)
    named = [routes_t[k : k + 1, :] == experts for k in range(2)]
    both = jnp.where(named[0] | named[1], 1.0, 0.0).astype(BF16)
    earlier = jnp.where(
        lax.broadcasted_iota(jnp.int32, (tokens, tokens), 0)
        < lax.broadcasted_iota(jnp.int32, (tokens, tokens), 1),
        1.0,
        0.0,
    ).astype(BF16)
    rank = jnp.dot(both, earlier, preferred_element_type=F32).astype(jnp.int32)
    place = lax.broadcasted_iota(jnp.int32, (expert_count, capacity, tokens), 1)
    rank = jnp.broadcast_to(rank[:, None, :], place.shape)
    masks = []
    for k in range(2):
        hit = jnp.broadcast_to(jnp.where(named[k], 1, 0)[:, None, :], place.shape)
        masks.append(((hit == 1) & (rank == place)).reshape(expert_count * capacity, tokens))
    return masks


def dispatch_kernel(which, rows_ref, gain_ref, routes_ref, normed_ref, packed_ref, *, experts, capacity):
    rows = rows_ref[...].astype(F32)
    inv = lax.rsqrt(jnp.mean(rows * rows, axis=-1, keepdims=True) + norm_eps)
    normed = (rows * inv * gain_ref[...]).astype(BF16)
    normed_ref[...] = normed
    first, second = slot_masks(routes_ref[...], experts, capacity)
    pick = jnp.where(first | second, 1.0, 0.0).astype(BF16)
    packed_ref[...] = jnp.dot(pick, normed, preferred_element_type=F32).astype(BF16)


def dispatch(tp_index, moe_input, ffn_gain, routes_t, own_count, experts, capacity):
    width = moe_input.shape[1]
    return pl.pallas_call(
        functools.partial(dispatch_kernel, experts=experts, capacity=capacity),
        grid_spec=pltpu.PrefetchScalarGridSpec(
            num_scalar_prefetch=1,
            grid=(1,),
            in_specs=[
                pl.BlockSpec((own_count, width), lambda i, w: (w[0], 0)),
                pl.BlockSpec((1, width), lambda i, w: (0, 0)),
                pl.BlockSpec((2, own_count), lambda i, w: (0, w[0])),
            ],
            out_specs=[
                pl.BlockSpec((own_count, width), lambda i, w: (0, 0)),
                pl.BlockSpec((experts * capacity, width), lambda i, w: (0, 0)),
            ],
        ),
        out_shape=[
            jax.ShapeDtypeStruct((own_count, width), BF16),
            jax.ShapeDtypeStruct((experts * capacity, width), BF16),
        ],
        compiler_params=pltpu.CompilerParams(vmem_limit_bytes=VMEM_LIMIT),
        name="dispatch",
    )(tp_index.reshape(1), moe_input, ffn_gain.reshape(1, -1), routes_t)


def combine_kernel(which, homed_ref, gates_ref, routes_ref, out_ref, *, experts, capacity):
    first, second = slot_masks(routes_ref[...], experts, capacity)
    gates = gates_ref[...]
    weights = jnp.where(first, gates[0:1, :], 0.0) + jnp.where(second, gates[1:2, :], 0.0)
    weights = weights.T
    high = weights.astype(BF16)
    low = (weights - high.astype(F32)).astype(BF16)
    homed = homed_ref[...]
    out = jnp.dot(high, homed, preferred_element_type=F32)
    out += jnp.dot(low, homed, preferred_element_type=F32)
    out_ref[...] = out.astype(BF16)


def combine(tp_index, homed, gates_t, routes_t, own_count, experts, capacity):
    width = homed.shape[1]
    return pl.pallas_call(
        functools.partial(combine_kernel, experts=experts, capacity=capacity),
        grid_spec=pltpu.PrefetchScalarGridSpec(
            num_scalar_prefetch=1,
            grid=(1,),
            in_specs=[
                pl.BlockSpec((experts * capacity, width), lambda i, w: (0, 0)),
                pl.BlockSpec((2, own_count), lambda i, w: (0, 0)),
                pl.BlockSpec((2, own_count), lambda i, w: (0, w[0])),
            ],
            out_specs=pl.BlockSpec((own_count, width), lambda i, w: (0, 0)),
        ),
        out_shape=jax.ShapeDtypeStruct((own_count, width), BF16),
        compiler_params=pltpu.CompilerParams(vmem_limit_bytes=VMEM_LIMIT),
        name="combine",
    )(tp_index.reshape(1), homed, gates_t, routes_t)


def route_gates(normed, own_routes, group_router, expert_router):
    group_count = group_router.shape[1]
    expert_count = expert_router.shape[1]
    group_logits = jnp.dot(normed, group_router, preferred_element_type=F32)
    expert_logits = jnp.dot(normed, expert_router, preferred_element_type=F32)
    chosen = own_routes[:, 0] // (expert_count // group_count)
    group_mask = jnp.arange(group_count, dtype=jnp.int32)[None, :] == chosen[:, None]
    own_logit = jnp.sum(jnp.where(group_mask, group_logits, 0.0), axis=-1, keepdims=True)
    group_share = 1.0 / jnp.sum(jnp.exp(group_logits - own_logit), axis=-1)
    expert_mask = jnp.arange(expert_count, dtype=jnp.int32)[None, None, :] == own_routes[:, :, None]
    picked = jnp.sum(jnp.where(expert_mask, expert_logits[:, None, :], 0.0), axis=-1)
    return group_share[:, None] * jax.nn.sigmoid(picked - picked[:, ::-1])


def call(body, args, outs, specs=None, prefetch=None):
    in_specs = [whole(a.shape) for a in args] if specs is None else specs
    out_specs = [whole(o.shape) for o in outs]
    grid_spec = pltpu.PrefetchScalarGridSpec(
        num_scalar_prefetch=0 if prefetch is None else 1,
        grid=(1,),
        in_specs=in_specs,
        out_specs=out_specs,
    )
    operands = args if prefetch is None else (prefetch, *args)
    return pl.pallas_call(
        body,
        grid_spec=grid_spec,
        out_shape=list(outs),
        compiler_params=pltpu.CompilerParams(vmem_limit_bytes=VMEM_LIMIT),
    )(*operands)


def pack_weights_kernel(gate_ref, up_ref, down_ref, top_ref, bottom_ref):
    rows, lanes = gate_ref.shape
    extra = top_ref.shape[0] - rows
    top_ref[:rows, :] = gate_ref[...]
    top_ref[rows:, :] = up_ref[:extra, :]
    bottom_ref[: rows - extra, :] = up_ref[extra:, :]
    at = rows - extra
    for n in range(down_ref.shape[1] // lanes):
        bottom_ref[at : at + lanes, :] = down_ref[:, n * lanes : (n + 1) * lanes]
        at += lanes


def pack_weights(gate, up, down):
    rows, lanes = gate.shape
    shape = jax.ShapeDtypeStruct((3 * rows // 2, lanes), BF16)
    return call(pack_weights_kernel, (gate, up, down), (shape, shape))


def ffn_kernel(*refs, parts):
    mine_ref, other_ref = refs[:2]
    tops, bottoms = refs[2 : 2 + parts], refs[2 + parts : 2 + 2 * parts]
    own_out, other_out = refs[2 + 2 * parts :]
    model = mine_ref.shape[1]
    lanes = tops[0].shape[1]
    extra = tops[0].shape[0] - model
    for rows_ref, out_ref in ((mine_ref, own_out), (other_ref, other_out)):
        rows = rows_ref[...]
        hidden = []
        for top, bottom in zip(tops, bottoms):
            gate = top[:model, :]
            up = jnp.concatenate([top[model:, :], bottom[: model - extra, :]], axis=0)
            gate_up = jnp.dot(
                rows, jnp.concatenate([gate, up], axis=1), preferred_element_type=F32
            )
            g, u = gate_up[:, :lanes], gate_up[:, lanes:]
            hidden.append((g / (1.0 + jnp.exp(-g)) * u).astype(BF16))
        hidden = jnp.concatenate(hidden, axis=1)
        for n in range(model // (2 * lanes)):
            at = model - extra + 2 * n * lanes
            block = jnp.concatenate(
                [
                    jnp.concatenate([b[at : at + lanes, :], b[at + lanes : at + 2 * lanes, :]], axis=1)
                    for b in bottoms
                ],
                axis=0,
            )
            out_ref[:, 2 * n * lanes : 2 * (n + 1) * lanes] = jnp.dot(
                hidden, block, preferred_element_type=F32
            ).astype(out_ref.dtype)


def ffn(mine, other, tops, bottoms):
    return call(
        functools.partial(ffn_kernel, parts=len(tops)),
        (mine, other, *tops, *bottoms),
        (jax.ShapeDtypeStruct(mine.shape, BF16), jax.ShapeDtypeStruct(mine.shape, BF16)),
    )


Q_CHUNK = 256
OFFSETS = (0, -1, 1, -2, 2, -3, 3, 4)


def pack_heads_kernel(where_ref, q_ref, k_ref, v_ref, *outs, half, depth):
    for n, out in enumerate(outs):
        pick = lax.rem(where_ref[1] - n + 4, 4)
        at = pl.ds(pl.multiple_of((pick // 2) * depth, depth), depth)
        rows = pl.ds(pl.multiple_of(lax.rem(pick, 2) * half, half), half)
        out[:, :depth] = k_ref[rows, at]
        out[:, depth : 2 * depth] = v_ref[rows, at]
        out[:, 2 * depth : 3 * depth] = q_ref[:half, at]
        out[:, 3 * depth :] = q_ref[half:, at]


def sort_heads_kernel(where_ref, *refs, half, depth):
    messages, (q_out, kv_out) = refs[:4], refs[4:]
    first = 2 * lax.rem(where_ref[1], 2) + where_ref[2]
    for n, message in enumerate(messages):
        at = pl.ds(pl.multiple_of(lax.rem(first + n, 4) * half, half), half)
        kv_out[at, :] = message[:, : 2 * depth]
        q_out[0, at, :] = message[:, 2 * depth : 3 * depth]
        q_out[1, at, :] = message[:, 3 * depth :]


def attend_kernel(where_ref, q_ref, *refs, slices, half, scale):
    blocks = refs[:slices]
    far_low = refs[slices]
    own_ref, other_ref, kv, acc, top_ref, sems = refs[slices + 1 :]
    z, core = where_ref[0], where_ref[2]
    keys, two_depth = blocks[0].shape
    depth = two_depth // 2
    width = depth // 2
    rows = q_ref.shape[1]
    copies = []
    for n, (offset, block) in enumerate(zip(OFFSETS, blocks)):
        source = lax.rem(z + offset + slices, slices) * keys
        copies.append(
            pltpu.make_async_copy(
                block, kv.at[pl.ds(pl.multiple_of(source, keys), block.shape[0]), :], sems.at[n]
            )
        )
        if n == slices - 1:
            copies.append(
                pltpu.make_async_copy(
                    far_low,
                    kv.at[
                        pl.ds(
                            pl.multiple_of(source + block.shape[0], block.shape[0]),
                            block.shape[0],
                        ),
                        :,
                    ],
                    sems.at[n + 1],
                )
            )
    for copy in copies:
        copy.start()
    for copy in copies:
        copy.wait()

    per_side = rows // Q_CHUNK

    def fold(q, first_key, count, q_first, q_half, diagonal):
        at = pl.ds(pl.multiple_of(first_key, keys), count)
        v = jnp.concatenate([kv[at, depth:], jnp.ones((count, depth), BF16)], axis=1)
        if diagonal:
            qi = lax.broadcasted_iota(jnp.int32, (Q_CHUNK, count), 0) + q_first
            ki = lax.broadcasted_iota(jnp.int32, (Q_CHUNK, count), 1)
            k_pos = (ki // half) * (2 * half) + core * half + ki % half
            q_pos = (qi // half) * (2 * half) + q_half * half + qi % half
            allowed = k_pos <= q_pos
        for m in range(2):
            s = lax.dot_general(
                q[:, m * width : (m + 1) * width],
                kv[at, m * width : (m + 1) * width],
                (((1,), (1,)), ((), ())),
                preferred_element_type=F32,
            )
            if diagonal:
                s = jnp.where(allowed, s, masked_score)
            top = jnp.max(s, axis=1, keepdims=True)
            if not diagonal:
                old = top_ref[m, :, :1]
                top = jnp.maximum(top, old)
                keep = jnp.exp2((old - top) * scale)
            e = jnp.exp2((s - top) * scale)
            if diagonal:
                e = jnp.where(allowed, e, 0.0)
            mixed = jnp.dot(e.astype(BF16), v, preferred_element_type=F32)
            if not diagonal:
                mixed = mixed + acc[m] * keep
            acc[m] = mixed
            top_ref[m] = jnp.broadcast_to(top, top_ref.shape[1:])

    def chunk(n, carry):
        side = n // per_side
        q_first = pl.multiple_of(lax.rem(n, per_side) * Q_CHUNK, Q_CHUNK)
        q_half = jnp.where(side == 0, core, 1 - core)
        q = q_ref[q_half, pl.ds(q_first, Q_CHUNK), :]
        fold(q, z * keys, keys, q_first, q_half, True)

        def pair(p, c):
            fold(q, p * 2 * keys, 2 * keys, q_first, q_half, False)
            return c

        lax.fori_loop(0, z // 2, pair, 0)

        @pl.when(lax.rem(z, 2) == 1)
        def _():
            fold(q, (z - 1) * keys, keys, q_first, q_half, False)

        at = pl.ds(q_first, Q_CHUNK)
        for chosen, ref in ((0, own_ref), (1, other_ref)):

            @pl.when(side == chosen)
            def _(ref=ref):
                for m in range(2):
                    ref[m, at, :depth] = acc[m, :, :depth]
                    ref[m, at, depth:] = jnp.concatenate(
                        [top_ref[m, :, : depth // 2], acc[m, :, depth : depth + depth // 2]], axis=1
                    )

        return carry

    lax.fori_loop(0, 2 * per_side, chunk, 0)


def attend(where, q, blocks, far_low, half, scale):
    rows, depth = q.shape[1:]
    slices = len(blocks)
    keys = blocks[0].shape[0]
    part = jax.ShapeDtypeStruct((2, rows, 2 * depth), F32)
    return pl.pallas_call(
        functools.partial(attend_kernel, slices=slices, half=half, scale=scale),
        grid_spec=pltpu.PrefetchScalarGridSpec(
            num_scalar_prefetch=1,
            grid=(1,),
            in_specs=[whole(q.shape)]
            + [pl.BlockSpec(memory_space=pl.ANY)] * (slices + 1),
            out_specs=[whole(part.shape)] * 2,
            scratch_shapes=[
                pltpu.VMEM((slices * keys, 2 * depth), BF16),
                pltpu.VMEM((2, Q_CHUNK, 2 * depth), F32),
                pltpu.VMEM((2, Q_CHUNK, depth), F32),
                pltpu.SemaphoreType.DMA((slices + 1,)),
            ],
        ),
        out_shape=[part, part],
        compiler_params=pltpu.CompilerParams(vmem_limit_bytes=VMEM_LIMIT),
        name="attend",
    )(where, q, *blocks, far_low)


def merge_kernel(where_ref, mine_ref, theirs_ref, weight_ref, gain_ref, *outs, scale):
    depth = gain_ref.shape[1]
    half = outs[0].shape[0]
    first = 2 * lax.rem(where_ref[1], 2) + where_ref[2]
    head = lax.rem(where_ref[1], 2)
    weight = jnp.where(where_ref[1] // 2 == where_ref[2], weight_ref[head], weight_ref[2 + head])
    for n, out_ref in enumerate(outs):
        at = pl.ds(pl.multiple_of(lax.rem(first + n, 4) * half, half), half)
        heads = []
        for m in range(2):
            mine, theirs = mine_ref[m, at, :], theirs_ref[m, at, :]
            top_a, top_b = mine[:, depth : depth + 1], theirs[:, depth : depth + 1]
            total_a = mine[:, depth + depth // 2 : depth + depth // 2 + 1]
            total_b = theirs[:, depth + depth // 2 : depth + depth // 2 + 1]
            top = jnp.maximum(top_a, top_b)
            keep_a = jnp.exp2((top_a - top) * scale)
            keep_b = jnp.exp2((top_b - top) * scale)
            total = total_a * keep_a + total_b * keep_b
            heads.append(mine[:, :depth] * (keep_a / total) + theirs[:, :depth] * (keep_b / total))
        out = heads[0] - weight * heads[1]
        out = out * lax.rsqrt(jnp.mean(out * out, axis=1, keepdims=True) + norm_eps)
        out_ref[...] = (out * gain_ref[...]).astype(BF16)


def merge(where, mine, theirs, weights, head_gain, half, scale):
    depth = head_gain.shape[0]
    args = (mine, theirs, weights, head_gain.reshape(1, depth))
    specs = [whole(a.shape) for a in args]
    specs[2] = pl.BlockSpec(memory_space=pltpu.SMEM)
    return call(
        functools.partial(merge_kernel, scale=scale),
        args,
        [jax.ShapeDtypeStruct((half, depth), BF16)] * 4,
        specs=specs,
        prefetch=where,
    )


def lay_out_kernel(where_ref, *refs):
    out = refs[4]
    half, depth = refs[0].shape
    for n, message in enumerate(refs[:4]):
        pick = lax.rem(where_ref[1] - n + 4, 4)
        rows = pl.ds(pl.multiple_of(lax.rem(pick, 2) * half, half), half)
        out[rows, pl.ds(pl.multiple_of((pick // 2) * depth, depth), depth)] = message[...]


def ring_pairs(step, size):
    pairs = []
    for target in range(size):
        source = (target - (1 if step > 0 else -1)) % size
        moved = (target - step) % size
        for hop in range(size):
            reader = (target + (hop if step > 0 else -hop)) % size
            distance = abs(step) + hop
            limit = 4
            if distance <= limit and moved < reader:
                pairs.append((source, target))
                break
    return pairs


def local(
    queries,
    keys,
    values,
    lambdas,
    head_gain,
    moe_input,
    ffn_gain,
    group_router,
    expert_router,
    routes,
    w_gate,
    w_up,
    w_down,
):
    z, x, _, core = (lax.axis_index(a) for a in EP_TP)
    tp_index = lax.axis_index(TP)
    where = jnp.stack([z, x, core])

    top, bottom = pack_weights(w_gate[0], w_up[0], w_down[0])
    top_f = shifted(top, "y", 1)
    bottom_b = shifted(bottom, "y", -1)
    bottom_f = shifted(bottom, "y", 1)
    top_b = shifted(top, "y", -1)
    top_o = shifted(top_f, "y", 1)
    bottom_o = shifted(bottom_b, "y", -1)

    rows = queries.shape[0]
    half = rows // 2
    depth = head_gain.shape[0]
    scale = math.log2(math.e) * (depth // 2) ** (-0.5)
    message = jax.ShapeDtypeStruct((half, 4 * depth), BF16)
    messages = call(
        functools.partial(pack_heads_kernel, half=half, depth=depth),
        (queries, keys, values),
        [message] * 4,
        prefetch=where,
    )

    def head_pairs(n, back=False):
        pairs = []
        for sx in range(4):
            for sc in range(2):
                pick = (sx - n) % 4
                here, there = sx * 2 + sc, (2 * sc + pick // 2) * 2 + pick % 2
                pairs.append((there, here) if back else (here, there))
        return pairs

    received = []
    for n, m in enumerate(messages):
        received.append(lax.ppermute(m, ("x", "c"), head_pairs(n)))
    q, kv = call(
        functools.partial(sort_heads_kernel, half=half, depth=depth),
        tuple(received),
        (
            jax.ShapeDtypeStruct((2, 4 * half, depth), BF16),
            jax.ShapeDtypeStruct((4 * half, 2 * depth), BF16),
        ),
        prefetch=where,
    )

    def ring(array, step):
        return lax.ppermute(array, "z", ring_pairs(step, lax.axis_size("z")))

    f1, b1 = ring(kv, 1), ring(kv, -1)
    f2, b2 = ring(f1, 2), ring(b1, -2)
    f3, b3 = ring(f2, 3), ring(b2, -3)
    mid = kv.shape[0] // 2
    far_high, far_low = ring(f3[:mid], 4), ring(b3[mid:], -4)
    all_lambdas = jnp.concatenate([lambdas, shifted(lambdas, "c", 1)])

    own_count = routes.shape[0] // lax.axis_size(TP)
    experts = expert_router.shape[1]
    capacity = 2 * own_count // experts
    model_width = moe_input.shape[1]
    routes_t = routes.T
    normed, packed = dispatch(tp_index, moe_input, ffn_gain, routes_t, own_count, experts, capacity)
    arrived = lax.all_to_all(
        packed.reshape(experts, capacity, model_width), EP, split_axis=0, concat_axis=0, tiled=True
    ).reshape(experts * capacity, model_width)
    other_rows = shifted(arrived, "c", 1)
    mine, theirs = ffn(
        arrived,
        other_rows,
        (top, top_f, top_b, top_o),
        (bottom, bottom_f, bottom_b, bottom_o),
    )
    results = mine + shifted(theirs, "c", 1)
    homed = lax.all_to_all(
        results.reshape(experts, capacity, model_width), EP, split_axis=0, concat_axis=0, tiled=True
    ).reshape(experts * capacity, model_width)

    part_own, part_other = attend(
        where, q, (kv, f1, b1, f2, b2, f3, b3, far_high), far_low, half, scale
    )
    part_got = shifted(part_other, "c", 1)
    outgoing = merge(where, part_own, part_got, all_lambdas, head_gain, half, scale)
    incoming = []
    for n, m in enumerate(outgoing):
        incoming.append(lax.ppermute(m, ("x", "c"), head_pairs(n, back=True)))
    (attn_out,) = call(
        lay_out_kernel,
        tuple(incoming),
        [jax.ShapeDtypeStruct((rows, queries.shape[1]), BF16)],
        prefetch=where,
    )

    own_routes = lax.dynamic_slice_in_dim(routes, tp_index * own_count, own_count, 0)
    gates = route_gates(normed, own_routes, group_router, expert_router)
    moe_out = combine(tp_index, homed, gates.T, routes_t, own_count, experts, capacity)
    return (attn_out, moe_out)


def solution(mesh):
    split = Mesh(mesh.devices.reshape(8, 4, 4, 2), EP_TP)
    placed = (
        P(EP, TP),
        P(EP, TP),
        P(EP, TP),
        P(TP),
        P(),
        P(EP, None),
        P(),
        P(),
        P(),
        P(EP, None),
        P(EP, None, TP),
        P(EP, None, TP),
        P(EP, TP, None),
    )

    return jax.shard_map(
        local, mesh=split, in_specs=placed, out_specs=(P(EP, TP), P(EP_TP, None)), check_vma=False
    )
```

time: 317 us -> 235 us (0.74)
  Pallas kernels: 0 us -> 56.7 us
  local copies, waits for them, and re-layouts: 50.8 us -> 6.74 us
  waiting for transfers between devices: 144 us -> 100 us
  matrix products: 38.5 us -> 0.52 us
  starting transfers between devices: 25.2 us -> 61.6 us
  other arithmetic: 25.1 us -> 4.16 us
  blocking collectives: 14.2 us -> 0 us
  between operations: 14.1 us -> 1.13 us
  loops' own time: 3.37 us -> 0 us
    all_gather x3 -> x0, waiting for transfers between devices: 144 us -> none  [the longest x1 61.7 us: in_one_piece(): whole, at, outs = (lax.all_gather(both, axis, axis=dim, tiled=True), 0, [])]
    ppermute x0 -> x26, waiting for transfers between devices: none -> 80.8 us  [the longest x8 35.8 us: ring(): return lax.ppermute(array, 'z', ring_pairs(step, lax.axis_size('z')))]
    pallas_call x0 -> x9, Pallas kernels: none -> 56.7 us  [the longest x1 28.7 us: attend(): pl.pallas_call(functools.partial(attend_kernel, slices=slices, half=half,...]
    ppermute x0 -> x26, starting transfers between devices: none -> 43.8 us  [the longest x8 17.6 us: ring(): return lax.ppermute(array, 'z', ring_pairs(step, lax.axis_size('z')))]
    dot_general x53 -> x2, matrix products: 38.5 us -> 0.52 us  [the longest x1 0.27 us: route_gates(): expert_logits = jnp.dot(normed, expert_router, preferred_element_type=F32)]
    dynamic_slice x32 -> x0, local copies, waits for them, and re-layouts: 32.8 us -> none  [the longest x16 17.2 us: value_compute(): lax.dynamic_slice_in_dim(value_shard, offset, value_block_rows, 0)]
    all_to_all x3 -> x2, waiting for transfers between devices: 0.01 us -> 19.6 us  [the longest x1 19.6 us: local(): lax.all_to_all(packed.reshape(experts, capacity, model_width), EP, split_...]
    all_gather x1 -> x0, blocking collectives: 14.2 us -> none  [gathered_by_axis(): array = lax.all_gather(array, axis, axis=dim, tiled=True)]
  transfers between devices with their start and end apart: 6 -> 28, of which waited for: 3 -> 14; matrix products, arithmetic and copies ran while one was open for 33% -> 2% of each run, Pallas kernels for 0% -> 19%
where the time goes in v1:
time: 235 us; the launch traced here: 231 us
  waiting for transfers between devices  100 us (43%)
  starting transfers between devices  61.6 us (26%)
  Pallas kernels  56.7 us (24%)
  local copies, waits for them, and re-layouts  6.74 us (3%)
  other arithmetic  4.16 us (2%)
    ppermute x8, waiting for transfers between devices, ring(): return lax.ppermute(array, 'z', ring_pairs(step, lax.axis_size('z')))  35.8 us
    ppermute x10, waiting for transfers between devices, shifted(): return lax.ppermute(array, axis, [(i, (i + by) % n) for i in range(n)])  35.6 us
    pallas_call x1, Pallas kernels, attend(): pl.pallas_call(functools.partial(attend_kernel, slices=slices, half=half,...  28.7 us
    pallas_call x6, Pallas kernels, call(): pl.pallas_call(body, grid_spec=grid_spec, out_shape=list(outs), compiler_...  22.6 us
    all_to_all x1, waiting for transfers between devices, local(): lax.all_to_all(packed.reshape(experts, capacity, model_width), EP, split_...  19.6 us
    ppermute x8, starting transfers between devices, ring(): return lax.ppermute(array, 'z', ring_pairs(step, lax.axis_size('z')))  17.6 us
    ppermute x4, starting transfers between devices, local(): incoming.append(lax.ppermute(m, ('x', 'c'), head_pairs(n, back=True)))  10.1 us
    ppermute x4, starting transfers between devices, local(): received.append(lax.ppermute(m, ('x', 'c'), head_pairs(n)))  9.76 us
  transfers between devices with their start and end apart: 28, of which 14 were waited for; matrix products, arithmetic and copies ran while one was open for 2% of the time, Pallas kernels for 19%

profile of v1, /device:TPU:238, one launch (start us, length us, event | category | flops | bytes accessed | tf_op | source)
XLA Modules:
  0.0 231.3 jit_solution(14364451590577141612)
XLA Ops:
  0.7 2.8 %dispatch.1 = (bf16[128,2048]{1,0:T(8,128)(2,1)}, bf16[256,2048]{1,0:T(8,128)(2,1)}) custom-call(s32[1]{0:T(128)} %bitcast.4.which, bf16[1024,2048]{1,0:T(8,128)(2,1)} %rows_ref.1, f32[1,2048]{1,0:T(1,128)} %bitcast.32, s32[2,1024]{1,0:T(2,128)} %bitcast.30), custom_call_target="tpu_custom_call" | custom-call | tf_op jit(solution)/shard_map/dispatch/pallas_call | solution.py:66
  3.4 8.5 %all-to-all-start = ((bf16[32,8,2048]{2,1,0:T(8,128)(2,1)}), bf16[32,8,2048]{2,1,0:T(8,128)(2,1)S(1)}, u32[]{:S(2)}, u32[]{:S(2)}) async-start(bf16[32,8,2048]{2,1,0:T(8,128)(2,1)} %bitcast.26), calls=%async_computation | async-start | bytes 2097152 | tf_op jit(solution)/shard_map/all_to_all | solution.py:507
  11.9 2.6 %shard_map.144 = (bf16[3072,128]{1,0:T(8,128)(2,1)}, bf16[3072,128]{1,0:T(8,128)(2,1)}) custom-call(bf16[2048,128]{1,0:T(8,128)(2,1)} %bitcast.27, bf16[2048,128]{1,0:T(8,128)(2,1)} %bitcast.28, bf16[128,2048]{1,0:T(8,128)(2,1)} %bitcast.29), custom_call_target="tpu_custom_call" | custom-call | tf_op jit(solution)/shard_map/pallas_call | solution.py:147
  16.5 19.6 %all-to-all-done = bf16[32,8,2048]{2,1,0:T(8,128)(2,1)S(1)} async-done(((bf16[32,8,2048]{2,1,0:T(8,128)(2,1)}), bf16[32,8,2048]{2,1,0:T(8,128)(2,1)S(1)}, u32[]{:S(2)}, u32[]{:S(2)}) %all-to-all-start) | async-done | bytes 1048608 | tf_op jit(solution)/shard_map/all_to_all | solution.py:507
  40.2 16.6 %collective-permute-done.20.refs_4_ = bf16[3072,128]{1,0:T(8,128)(2,1)S(1)} collective-permute-done((bf16[3072,128]{1,0:T(8,128)(2,1)}, bf16[3072,128]{1,0:T(8,128)(2,1)S(1)}, u32[]{:S(2)}, u32[]{:S(2)}) %collective-permute-start.20) | collective-permute-done | bytes 786464 | tf_op jit(solution)/shard_map/ppermute | solution.py:26
  58.2 16.4 %collective-permute-done.21.refs_5_ = bf16[3072,128]{1,0:T(8,128)(2,1)S(1)} collective-permute-done((bf16[3072,128]{1,0:T(8,128)(2,1)S(1)}, bf16[3072,128]{1,0:T(8,128)(2,1)S(1)}, u32[]{:S(2)}, u32[]{:S(2)}) %collective-permute-start.21) | collective-permute-done | bytes 786464 | tf_op jit(solution)/shard_map/ppermute | solution.py:26
  76.8 7.9 %shard_map.145 = (bf16[256,2048]{1,0:T(8,128)(2,1)}, bf16[256,2048]{1,0:T(8,128)(2,1)}) custom-call(bf16[256,2048]{1,0:T(8,128)(2,1)} %bitcast.25, bf16[256,2048]{1,0:T(8,128)(2,1)} %copy-done.5, bf16[3072,128]{1,0:T(8,128)(2,1)} %get-tuple-element.33.refs_2_, bf16[3072,128]{1,0:T(8,128)(2,1)} %copy-done.6, bf16[3072,128]{1,0:T(8,128)(2,1)} %copy-done.8, ...), custom_call_target="tpu_custom_call" | custom-call | tf_op jit(solution)/shard_map/pallas_call | solution.py:147
  87.9 3.2 %collective-permute-start = (bf16[128,512]{1,0:T(8,128)(2,1)}, bf16[128,512]{1,0:T(8,128)(2,1)S(1)}, u32[]{:S(2)}, u32[]{:S(2)}) collective-permute-start(bf16[128,512]{1,0:T(8,128)(2,1)} %get-tuple-element.20), channel_id=1, source_target_pairs={{0,0},{1,16},{8,1},{9,17},{16,8},{17,24},{24,9},{25,25},{2,2},{3,1... | collective-permute-start | bytes 393224 | tf_op jit(solution)/shard_map/ppermute | solution.py:480
  91.1 4.0 %collective-permute-start.1 = (bf16[128,512]{1,0:T(8,128)(2,1)}, bf16[128,512]{1,0:T(8,128)(2,1)S(1)}, u32[]{:S(2)}, u32[]{:S(2)}) collective-permute-start(bf16[128,512]{1,0:T(8,128)(2,1)} %get-tuple-element.21), channel_id=1, source_target_pairs={{0,9},{1,25},{8,0},{9,16},{16,1},{17,17},{24,8},{25,24},{2,11},{3,... | collective-permute-start | bytes 393224 | tf_op jit(solution)/shard_map/ppermute | solution.py:480
  98.0 3.1 %collective-permute-done.2.refs_2_ = bf16[128,512]{1,0:T(8,128)(2,1)S(1)} collective-permute-done((bf16[128,512]{1,0:T(8,128)(2,1)}, bf16[128,512]{1,0:T(8,128)(2,1)S(1)}, u32[]{:S(2)}, u32[]{:S(2)}) %collective-permute-start.2) | collective-permute-done | bytes 131104 | tf_op jit(solution)/shard_map/ppermute | solution.py:480
  103.9 2.6 %shard_map.141 = (bf16[2,512,128]{2,1,0:T(8,128)(2,1)}, bf16[512,256]{1,0:T(8,128)(2,1)}) custom-call(s32[3]{0:T(128)} %pad_add_fusion.where_ref, bf16[128,512]{1,0:T(8,128)(2,1)} %copy-done.18, bf16[128,512]{1,0:T(8,128)(2,1)} %copy-done.20, bf16[128,512]{1,0:T(8,128)(2,1)} %copy-done.21, bf16[128,512]{1,0:T(8,128)(2,1)} %copy-done.23), custom_call_target="tpu_custom_call" | custom-call | tf_op jit(solution)/shard_map/pallas_call | solution.py:147
  109.1 6.8 %collective-permute-done.4.refs_1_ = bf16[512,256]{1,0:T(8,128)(2,1)S(1)} collective-permute-done((bf16[512,256]{1,0:T(8,128)(2,1)}, bf16[512,256]{1,0:T(8,128)(2,1)S(1)}, u32[]{:S(2)}, u32[]{:S(2)}) %collective-permute-start.4) | collective-permute-done | bytes 262176 | tf_op jit(solution)/shard_map/ppermute | solution.py:492
  117.2 3.1 %collective-permute-done.5.refs_2_ = bf16[512,256]{1,0:T(8,128)(2,1)S(1)} collective-permute-done((bf16[512,256]{1,0:T(8,128)(2,1)}, bf16[512,256]{1,0:T(8,128)(2,1)S(1)}, u32[]{:S(2)}, u32[]{:S(2)}) %collective-permute-start.5) | collective-permute-done | bytes 262176 | tf_op jit(solution)/shard_map/ppermute | solution.py:492
  124.6 9.4 %all-to-all-start.1 = ((bf16[32,8,2048]{2,1,0:T(8,128)(2,1)}), bf16[32,8,2048]{2,1,0:T(8,128)(2,1)S(1)}, u32[]{:S(2)}, u32[]{:S(2)}) async-start(bf16[32,8,2048]{2,1,0:T(8,128)(2,1)} %add_bitcast_fusion), calls=%async_computation.1 | async-start | bytes 2097152 | tf_op jit(solution)/shard_map/all_to_all | solution.py:518
  135.5 4.6 %collective-permute-start.9 = (bf16[512,256]{1,0:T(8,128)(2,1)S(1)}, bf16[512,256]{1,0:T(8,128)(2,1)S(1)}, u32[]{:S(2)}, u32[]{:S(2)}) collective-permute-start(bf16[512,256]{1,0:T(8,128)(2,1)S(1)} %collective-permute-done.7.refs_4_), channel_id=1, source_target_pairs={{32,0},{192,160},{224,192},{0,224},{33,1},{193,161},{225,193},{1,2... | collective-permute-start | bytes 786440 | tf_op jit(solution)/shard_map/ppermute | solution.py:492
  140.1 22.6 %collective-permute-done.8.refs_5_ = bf16[512,256]{1,0:T(8,128)(2,1)S(1)} collective-permute-done((bf16[512,256]{1,0:T(8,128)(2,1)S(1)}, bf16[512,256]{1,0:T(8,128)(2,1)S(1)}, u32[]{:S(2)}, u32[]{:S(2)}) %collective-permute-start.8) | collective-permute-done | bytes 262176 | tf_op jit(solution)/shard_map/ppermute | solution.py:492
  164.1 4.6 %collective-permute-start.11 = (bf16[256,256]{1,0:T(8,128)(2,1)S(1)}, bf16[256,256]{1,0:T(8,128)(2,1)S(1)}, u32[]{:S(2)}, u32[]{:S(2)}) collective-permute-start(bf16[256,256]{1,0:T(8,128)(2,1)S(1)} %slice.13), channel_id=1, source_target_pairs={{160,128},{192,160},{224,192},{0,224},{161,129},{193,161},{225,193... | collective-permute-start | bytes 393224 | tf_op jit(solution)/shard_map/ppermute | solution.py:492
  169.6 2.5 %collective-permute-done.11.refs_8_ = bf16[256,256]{1,0:T(8,128)(2,1)S(1)} collective-permute-done((bf16[256,256]{1,0:T(8,128)(2,1)S(1)}, bf16[256,256]{1,0:T(8,128)(2,1)S(1)}, u32[]{:S(2)}, u32[]{:S(2)}) %collective-permute-start.11) | collective-permute-done | bytes 131104 | tf_op jit(solution)/shard_map/ppermute | solution.py:492
  172.8 28.7 %attend.1 = (f32[2,512,256]{2,1,0:T(8,128)}, f32[2,512,256]{2,1,0:T(8,128)}) custom-call(s32[3]{0:T(128)} %pad_add_fusion.where_ref, bf16[2,512,128]{2,1,0:T(8,128)(2,1)} %get-tuple-element.24.q_ref, bf16[512,256]{1,0:T(8,128)(2,1)} %get-tuple-element.25.refs_0_, bf16[512,256]{1,0:T(8,128)(2,1)} %copy-done.14, bf16[512,256]{1,0:T(8,128)(2,1)} %copy-done.15, ...), custom_call_target="tpu_custom_call" | custom-call | tf_op jit(solution)/shard_map/attend/pallas_call | solution.py:347
  205.4 4.8 %shard_map.142 = (bf16[128,128]{1,0:T(8,128)(2,1)}, bf16[128,128]{1,0:T(8,128)(2,1)}, bf16[128,128]{1,0:T(8,128)(2,1)}, bf16[128,128]{1,0:T(8,128)(2,1)}) custom-call(s32[3]{0:T(128)} %pad_add_fusion.where_ref, f32[2,512,256]{2,1,0:T(8,128)} %get-tuple-element.26.mine_ref, f32[2,512,256]{2,1,0:T(8,128)} %copy-done.4, f32[4]{0:T(128)} %pad_maximum_fusion.weight_ref, ...), custom_call_target="tpu_custom_call" | custom-call | tf_op jit(solution)/shard_map/pallas_call | solution.py:147
  214.7 3.0 %collective-permute-start.16 = (bf16[128,128]{1,0:T(8,128)(2,1)}, bf16[128,128]{1,0:T(8,128)(2,1)S(1)}, u32[]{:S(2)}, u32[]{:S(2)}) collective-permute-start(bf16[128,128]{1,0:T(8,128)(2,1)} %get-tuple-element.30), channel_id=1, source_target_pairs={{8,0},{24,1},{9,8},{25,9},{0,16},{16,17},{1,24},{17,25},{10,2},{26... | collective-permute-start | bytes 98312 | tf_op jit(solution)/shard_map/ppermute | solution.py:529
  217.6 2.6 %collective-permute-start.17 = (bf16[128,128]{1,0:T(8,128)(2,1)}, bf16[128,128]{1,0:T(8,128)(2,1)S(1)}, u32[]{:S(2)}, u32[]{:S(2)}) collective-permute-start(bf16[128,128]{1,0:T(8,128)(2,1)} %get-tuple-element.31), channel_id=1, source_target_pairs={{1,0},{17,1},{8,8},{24,9},{9,16},{25,17},{0,24},{16,25},{3,2},{19,... | collective-permute-start | bytes 98312 | tf_op jit(solution)/shard_map/ppermute | solution.py:529
  220.9 4.0 %collective-permute-done.17.refs_3_ = bf16[128,128]{1,0:T(8,128)(2,1)S(1)} collective-permute-done((bf16[128,128]{1,0:T(8,128)(2,1)}, bf16[128,128]{1,0:T(8,128)(2,1)S(1)}, u32[]{:S(2)}, u32[]{:S(2)}) %collective-permute-start.17) | collective-permute-done | bytes 32800 | tf_op jit(solution)/shard_map/ppermute | solution.py:529
  228.7 2.7 %combine.1 = bf16[128,2048]{1,0:T(8,128)(2,1)} custom-call(s32[1]{0:T(128)} %bitcast.4.which, bf16[256,2048]{1,0:T(8,128)(2,1)} %bitcast.23, f32[2,128]{1,0:T(2,128)} %multiply_bitcast_fusion.gates_ref, s32[2,1024]{1,0:T(2,128)} %bitcast.31), custom_call_target="tpu_custom_call" | custom-call | tf_op jit(solution)/shard_map/combine/pallas_call | solution.py:105
  (115 shorter events, 43.7 us)
Async XLA Ops:
  3.4 32.7 %all-to-all-start = ((bf16[32,8,2048]{2,1,0:T(8,128)(2,1)}), bf16[32,8,2048]{2,1,0:T(8,128)(2,1)S(1)}, u32[]{:S(2)}, u32[]{:S(2)}) async-start(bf16[32,8,2048]{2,1,0:T(8,128)(2,1)} %bitcast.26), calls=%async_computation | async-start | bytes 2097152 | tf_op jit(solution)/shard_map/all_to_all | solution.py:507
  14.5 23.7 %collective-permute-start.19 = (bf16[3072,128]{1,0:T(8,128)(2,1)}, bf16[3072,128]{1,0:T(8,128)(2,1)S(1)}, u32[]{:S(2)}, u32[]{:S(2)}) collective-permute-start(bf16[3072,128]{1,0:T(8,128)(2,1)} %get-tuple-element.33.refs_2_), channel_id=1, source_target_pairs={{0,2},{2,4},{4,6},{6,0},{1,3},{3,5},{5,7},{7,1},{8,10},{10,12},{12... | collective-permute-start | bytes 2359304 | tf_op jit(solution)/shard_map/ppermute | solution.py:26
  16.1 23.7 %collective-permute-start.23 = (bf16[3072,128]{1,0:T(8,128)(2,1)}, bf16[3072,128]{1,0:T(8,128)(2,1)S(1)}, u32[]{:S(2)}, u32[]{:S(2)}) collective-permute-start(bf16[3072,128]{1,0:T(8,128)(2,1)} %get-tuple-element.34.refs_6_), channel_id=1, source_target_pairs={{0,6},{2,0},{4,2},{6,4},{1,7},{3,1},{5,3},{7,5},{8,14},{10,8},{12,... | collective-permute-start | bytes 2359304 | tf_op jit(solution)/shard_map/ppermute | solution.py:26
  36.2 38.5 %collective-permute-start.18 = (bf16[256,2048]{1,0:T(8,128)(2,1)S(1)}, bf16[256,2048]{1,0:T(8,128)(2,1)S(1)}, u32[]{:S(2)}, u32[]{:S(2)}) collective-permute-start(bf16[256,2048]{1,0:T(8,128)(2,1)S(1)} %bitcast.24), channel_id=1, source_target_pairs={{0,1},{1,0},{2,3},{3,2},{4,5},{5,4},{6,7},{7,6},{8,9},{9,8},{10,11... | collective-permute-start | bytes 3145736 | tf_op jit(solution)/shard_map/ppermute | solution.py:26
  36.2 20.6 %collective-permute-start.20 = (bf16[3072,128]{1,0:T(8,128)(2,1)}, bf16[3072,128]{1,0:T(8,128)(2,1)S(1)}, u32[]{:S(2)}, u32[]{:S(2)}) collective-permute-start(bf16[3072,128]{1,0:T(8,128)(2,1)} %get-tuple-element.33.refs_2_), channel_id=1, source_target_pairs={{0,6},{2,0},{4,2},{6,4},{1,7},{3,1},{5,3},{7,5},{8,14},{10,8},{12,... | collective-permute-start | bytes 2359304 | tf_op jit(solution)/shard_map/ppermute | solution.py:26
  36.6 21.6 %collective-permute-start.22 = (bf16[3072,128]{1,0:T(8,128)(2,1)}, bf16[3072,128]{1,0:T(8,128)(2,1)S(1)}, u32[]{:S(2)}, u32[]{:S(2)}) collective-permute-start(bf16[3072,128]{1,0:T(8,128)(2,1)} %get-tuple-element.34.refs_6_), channel_id=1, source_target_pairs={{0,2},{2,4},{4,6},{6,0},{1,3},{3,5},{5,7},{7,1},{8,10},{10,12},{12... | collective-permute-start | bytes 2359304 | tf_op jit(solution)/shard_map/ppermute | solution.py:26
  38.2 36.4 %collective-permute-start.21 = (bf16[3072,128]{1,0:T(8,128)(2,1)S(1)}, bf16[3072,128]{1,0:T(8,128)(2,1)S(1)}, u32[]{:S(2)}, u32[]{:S(2)}) collective-permute-start(bf16[3072,128]{1,0:T(8,128)(2,1)S(1)} %collective-permute-done.19.refs_3_), channel_id=1, source_target_pairs={{0,2},{2,4},{4,6},{6,0},{1,3},{3,5},{5,7},{7,1},{8,10},{10,12},{12... | collective-permute-start | bytes 2359304 | tf_op jit(solution)/shard_map/ppermute | solution.py:26
  39.8 34.8 %collective-permute-start.24 = (bf16[3072,128]{1,0:T(8,128)(2,1)S(1)}, bf16[3072,128]{1,0:T(8,128)(2,1)S(1)}, u32[]{:S(2)}, u32[]{:S(2)}) collective-permute-start(bf16[3072,128]{1,0:T(8,128)(2,1)S(1)} %collective-permute-done.23.refs_8_), channel_id=1, source_target_pairs={{0,6},{2,0},{4,2},{6,4},{1,7},{3,1},{5,3},{7,5},{8,14},{10,8},{12,... | collective-permute-start | bytes 2359304 | tf_op jit(solution)/shard_map/ppermute | solution.py:26
  84.7 37.5 %collective-permute-start.25 = (bf16[256,2048]{1,0:T(8,128)(2,1)}, bf16[256,2048]{1,0:T(8,128)(2,1)S(1)}, u32[]{:S(2)}, u32[]{:S(2)}) collective-permute-start(bf16[256,2048]{1,0:T(8,128)(2,1)} %get-tuple-element.36), channel_id=1, source_target_pairs={{0,1},{1,0},{2,3},{3,2},{4,5},{5,4},{6,7},{7,6},{8,9},{9,8},{10,11... | collective-permute-start | bytes 3145736 | tf_op jit(solution)/shard_map/ppermute | solution.py:26
  87.9 9.8 %collective-permute-start = (bf16[128,512]{1,0:T(8,128)(2,1)}, bf16[128,512]{1,0:T(8,128)(2,1)S(1)}, u32[]{:S(2)}, u32[]{:S(2)}) collective-permute-start(bf16[128,512]{1,0:T(8,128)(2,1)} %get-tuple-element.20), channel_id=1, source_target_pairs={{0,0},{1,16},{8,1},{9,17},{16,8},{17,24},{24,9},{25,25},{2,2},{3,1... | collective-permute-start | bytes 393224 | tf_op jit(solution)/shard_map/ppermute | solution.py:480
  95.2 8.0 %collective-permute-start.3 = (bf16[128,512]{1,0:T(8,128)(2,1)}, bf16[128,512]{1,0:T(8,128)(2,1)S(1)}, u32[]{:S(2)}, u32[]{:S(2)}) collective-permute-start(bf16[128,512]{1,0:T(8,128)(2,1)} %get-tuple-element.23), channel_id=1, source_target_pairs={{0,1},{1,17},{8,8},{9,24},{16,9},{17,25},{24,0},{25,16},{2,3},{3,1... | collective-permute-start | bytes 393224 | tf_op jit(solution)/shard_map/ppermute | solution.py:480
  106.5 9.4 %collective-permute-start.4 = (bf16[512,256]{1,0:T(8,128)(2,1)}, bf16[512,256]{1,0:T(8,128)(2,1)S(1)}, u32[]{:S(2)}, u32[]{:S(2)}) collective-permute-start(bf16[512,256]{1,0:T(8,128)(2,1)} %get-tuple-element.25.refs_0_), channel_id=1, source_target_pairs={{0,32},{32,64},{64,96},{96,128},{128,160},{160,192},{192,224},{1,3... | collective-permute-start | bytes 786440 | tf_op jit(solution)/shard_map/ppermute | solution.py:492
  107.8 12.5 %collective-permute-start.5 = (bf16[512,256]{1,0:T(8,128)(2,1)}, bf16[512,256]{1,0:T(8,128)(2,1)S(1)}, u32[]{:S(2)}, u32[]{:S(2)}) collective-permute-start(bf16[512,256]{1,0:T(8,128)(2,1)} %get-tuple-element.25.refs_0_), channel_id=1, source_target_pairs={{32,0},{64,32},{96,64},{0,224},{33,1},{65,33},{97,65},{1,225},{34,... | collective-permute-start | bytes 786440 | tf_op jit(solution)/shard_map/ppermute | solution.py:492
  115.9 18.0 %collective-permute-start.6 = (bf16[512,256]{1,0:T(8,128)(2,1)S(1)}, bf16[512,256]{1,0:T(8,128)(2,1)S(1)}, u32[]{:S(2)}, u32[]{:S(2)}) collective-permute-start(bf16[512,256]{1,0:T(8,128)(2,1)S(1)} %collective-permute-done.4.refs_1_), channel_id=1, source_target_pairs={{32,64},{64,96},{96,128},{128,160},{160,192},{192,224},{33,65},{65... | collective-permute-start | bytes 786440 | tf_op jit(solution)/shard_map/ppermute | solution.py:492
  120.3 15.2 %collective-permute-start.7 = (bf16[512,256]{1,0:T(8,128)(2,1)S(1)}, bf16[512,256]{1,0:T(8,128)(2,1)S(1)}, u32[]{:S(2)}, u32[]{:S(2)}) collective-permute-start(bf16[512,256]{1,0:T(8,128)(2,1)S(1)} %collective-permute-done.5.refs_2_), channel_id=1, source_target_pairs={{32,0},{64,32},{224,192},{0,224},{33,1},{65,33},{225,193},{1,225},... | collective-permute-start | bytes 786440 | tf_op jit(solution)/shard_map/ppermute | solution.py:492
  124.6 103.1 %all-to-all-start.1 = ((bf16[32,8,2048]{2,1,0:T(8,128)(2,1)}), bf16[32,8,2048]{2,1,0:T(8,128)(2,1)S(1)}, u32[]{:S(2)}, u32[]{:S(2)}) async-start(bf16[32,8,2048]{2,1,0:T(8,128)(2,1)} %add_bitcast_fusion), calls=%async_computation.1 | async-start | bytes 2097152 | tf_op jit(solution)/shard_map/all_to_all | solution.py:518
  134.0 28.8 %collective-permute-start.8 = (bf16[512,256]{1,0:T(8,128)(2,1)S(1)}, bf16[512,256]{1,0:T(8,128)(2,1)S(1)}, u32[]{:S(2)}, u32[]{:S(2)}) collective-permute-start(bf16[512,256]{1,0:T(8,128)(2,1)S(1)} %collective-permute-done.6.refs_3_), channel_id=1, source_target_pairs={{64,96},{96,128},{128,160},{160,192},{192,224},{65,97},{97,129},{1... | collective-permute-start | bytes 786440 | tf_op jit(solution)/shard_map/ppermute | solution.py:492
  135.5 28.6 %collective-permute-start.9 = (bf16[512,256]{1,0:T(8,128)(2,1)S(1)}, bf16[512,256]{1,0:T(8,128)(2,1)S(1)}, u32[]{:S(2)}, u32[]{:S(2)}) collective-permute-start(bf16[512,256]{1,0:T(8,128)(2,1)S(1)} %collective-permute-done.7.refs_4_), channel_id=1, source_target_pairs={{32,0},{192,160},{224,192},{0,224},{33,1},{193,161},{225,193},{1,2... | collective-permute-start | bytes 786440 | tf_op jit(solution)/shard_map/ppermute | solution.py:492
  140.0 62.6 %collective-permute-start.13 = (f32[2]{0:T(128)S(1)}, f32[2]{0:T(128)S(1)}, u32[]{:S(2)}, u32[]{:S(2)}) collective-permute-start(f32[2]{0:T(128)S(1)} %copy-done.29), channel_id=1, source_target_pairs={{0,1},{1,0},{2,3},{3,2},{4,5},{5,4},{6,7},{7,6},{8,9},{9,8},{10,11... | collective-permute-start | bytes 32 | tf_op jit(solution)/shard_map/ppermute | solution.py:26
  162.8 6.9 %collective-permute-start.10 = (bf16[256,256]{1,0:T(8,128)(2,1)S(1)}, bf16[256,256]{1,0:T(8,128)(2,1)S(1)}, u32[]{:S(2)}, u32[]{:S(2)}) collective-permute-start(bf16[256,256]{1,0:T(8,128)(2,1)S(1)} %slice.12), channel_id=1, source_target_pairs={{96,128},{128,160},{160,192},{192,224},{97,129},{129,161},{161,193... | collective-permute-start | bytes 393224 | tf_op jit(solution)/shard_map/ppermute | solution.py:492
  164.1 8.1 %collective-permute-start.11 = (bf16[256,256]{1,0:T(8,128)(2,1)S(1)}, bf16[256,256]{1,0:T(8,128)(2,1)S(1)}, u32[]{:S(2)}, u32[]{:S(2)}) collective-permute-start(bf16[256,256]{1,0:T(8,128)(2,1)S(1)} %slice.13), channel_id=1, source_target_pairs={{160,128},{192,160},{224,192},{0,224},{161,129},{193,161},{225,193... | collective-permute-start | bytes 393224 | tf_op jit(solution)/shard_map/ppermute | solution.py:492
  210.2 10.7 %collective-permute-start.14 = (bf16[128,128]{1,0:T(8,128)(2,1)}, bf16[128,128]{1,0:T(8,128)(2,1)S(1)}, u32[]{:S(2)}, u32[]{:S(2)}) collective-permute-start(bf16[128,128]{1,0:T(8,128)(2,1)} %get-tuple-element.28), channel_id=1, source_target_pairs={{0,0},{16,1},{1,8},{17,9},{8,16},{24,17},{9,24},{25,25},{2,2},{18,... | collective-permute-start | bytes 98312 | tf_op jit(solution)/shard_map/ppermute | solution.py:529
  212.8 8.1 %collective-permute-start.15 = (bf16[128,128]{1,0:T(8,128)(2,1)}, bf16[128,128]{1,0:T(8,128)(2,1)S(1)}, u32[]{:S(2)}, u32[]{:S(2)}) collective-permute-start(bf16[128,128]{1,0:T(8,128)(2,1)} %get-tuple-element.29), channel_id=1, source_target_pairs={{9,0},{25,1},{0,8},{16,9},{1,16},{17,17},{8,24},{24,25},{11,2},{27... | collective-permute-start | bytes 98312 | tf_op jit(solution)/shard_map/ppermute | solution.py:529
  217.6 7.2 %collective-permute-start.17 = (bf16[128,128]{1,0:T(8,128)(2,1)}, bf16[128,128]{1,0:T(8,128)(2,1)S(1)}, u32[]{:S(2)}, u32[]{:S(2)}) collective-permute-start(bf16[128,128]{1,0:T(8,128)(2,1)} %get-tuple-element.31), channel_id=1, source_target_pairs={{1,0},{17,1},{8,8},{24,9},{9,16},{25,17},{0,24},{16,25},{3,2},{19,... | collective-permute-start | bytes 98312 | tf_op jit(solution)/shard_map/ppermute | solution.py:529
  (34 other events, 788.9 us)

commit v2 on v0

v2 whole, which is shorter than its diff:
```python
import functools
import math

import jax
import jax.numpy as jnp
from jax import lax
from jax.experimental import pallas as pl
from jax.experimental.pallas import tpu as pltpu
from jax.sharding import Mesh
from jax.sharding import PartitionSpec as P


EP = ("z", "x")
EP_TP = ("z", "x", "y", "c")
TP = ("y", "c")

norm_eps = 1e-06
masked_score = -1e30
F32 = jnp.float32
BF16 = jnp.bfloat16
WIDE = 56 * 1024 * 1024


def shifted(array, axis, by):
    n = lax.axis_size(axis)
    return lax.ppermute(array, axis, [(i, (i + by) % n) for i in range(n)])


def windowed(body, args, outs, scalars, specs=None):
    def whole(shape):
        return pl.BlockSpec(shape, lambda *_: (0,) * len(shape))

    return pl.pallas_call(
        body,
        grid_spec=pltpu.PrefetchScalarGridSpec(
            num_scalar_prefetch=len(scalars),
            grid=(1,),
            in_specs=[whole(a.shape) for a in args] if specs is None else specs,
            out_specs=[whole(o.shape) for o in outs],
        ),
        out_shape=list(outs),
        compiler_params=pltpu.CompilerParams(vmem_limit_bytes=WIDE),
    )(*scalars, *args)


def call(body, args, outs, scalars=(), streamed=(), scratch=(), vmem=8 * 1024 * 1024):
    return pl.pallas_call(
        body,
        in_specs=[pl.BlockSpec(memory_space=pltpu.SMEM)] * len(scalars)
        + [pl.BlockSpec(memory_space=pltpu.HBM)] * len(streamed)
        + [pl.BlockSpec(memory_space=pltpu.VMEM)] * len(args),
        out_specs=[pl.BlockSpec(memory_space=pltpu.VMEM)] * len(outs),
        out_shape=list(outs),
        scratch_shapes=list(scratch),
        compiler_params=pltpu.CompilerParams(vmem_limit_bytes=vmem),
    )(*scalars, *streamed, *args)


def slot_masks(routes_t, expert_count, capacity):
    tokens = routes_t.shape[1]
    experts = lax.broadcasted_iota(jnp.int32, (expert_count, tokens), 0)
    named = [routes_t[k : k + 1, :] == experts for k in range(2)]
    both = jnp.where(named[0] | named[1], 1.0, 0.0).astype(BF16)
    earlier = jnp.where(
        lax.broadcasted_iota(jnp.int32, (tokens, tokens), 0)
        < lax.broadcasted_iota(jnp.int32, (tokens, tokens), 1),
        1.0,
        0.0,
    ).astype(BF16)
    rank = jnp.dot(both, earlier, preferred_element_type=F32).astype(jnp.int32)
    place = lax.broadcasted_iota(jnp.int32, (expert_count, capacity, tokens), 1)
    rank = jnp.broadcast_to(rank[:, None, :], place.shape)
    masks = []
    for k in range(2):
        hit = jnp.broadcast_to(jnp.where(named[k], 1, 0)[:, None, :], place.shape)
        masks.append(((hit == 1) & (rank == place)).reshape(expert_count * capacity, tokens))
    return masks


def own_routes(tp_ref, routes_ref, own_count):
    return routes_ref[:, pl.ds(pl.multiple_of(tp_ref[0] * own_count, own_count), own_count)]


def dispatch_kernel(
    tp_ref, rows_ref, gain_ref, routes_ref, normed_ref, packed_ref, *, experts, capacity
):
    rows = rows_ref[...].astype(F32)
    inv = lax.rsqrt(jnp.mean(rows * rows, axis=-1, keepdims=True) + norm_eps)
    normed = (rows * inv * gain_ref[...]).astype(BF16)
    normed_ref[...] = normed
    first, second = slot_masks(routes_ref[...], experts, capacity)
    pick = jnp.where(first | second, 1.0, 0.0).astype(BF16)
    packed_ref[...] = jnp.dot(pick, normed, preferred_element_type=F32).astype(BF16)


def dispatch(tp, moe_input, ffn_gain, routes_t, own_count, experts, capacity):
    width = moe_input.shape[1]
    return windowed(
        functools.partial(dispatch_kernel, experts=experts, capacity=capacity),
        (moe_input, ffn_gain.reshape(1, -1), routes_t),
        (
            jax.ShapeDtypeStruct((own_count, width), BF16),
            jax.ShapeDtypeStruct((experts * capacity, width), BF16),
        ),
        (tp,),
        [
            pl.BlockSpec((own_count, width), lambda i, t: (t[0], 0)),
            pl.BlockSpec((1, width), lambda i, t: (0, 0)),
            pl.BlockSpec((2, own_count), lambda i, t: (0, t[0])),
        ],
    )


def combine_kernel(tp_ref, homed_ref, gates_ref, routes_ref, out_ref, *, experts, capacity):
    own_count = out_ref.shape[0]
    first, second = slot_masks(own_routes(tp_ref, routes_ref, own_count), experts, capacity)
    gates = gates_ref[...]
    weights = jnp.where(first, gates[0:1, :], 0.0) + jnp.where(second, gates[1:2, :], 0.0)
    weights = weights.T
    high = weights.astype(BF16)
    low = (weights - high.astype(F32)).astype(BF16)
    homed = homed_ref[...]
    out = jnp.dot(high, homed, preferred_element_type=F32)
    out += jnp.dot(low, homed, preferred_element_type=F32)
    out_ref[...] = out.astype(BF16)


def combine(tp, homed, gates_t, routes_t, own_count, experts, capacity):
    (out,) = call(
        functools.partial(combine_kernel, experts=experts, capacity=capacity),
        (homed, gates_t, routes_t),
        (jax.ShapeDtypeStruct((own_count, homed.shape[1]), BF16),),
        scalars=(tp,),
    )
    return out


def gates_kernel(tp_ref, normed_ref, groups_ref, experts_ref, routes_ref, out_ref):
    normed = normed_ref[...]
    group_logits, expert_logits = (
        lax.dot_general(
            ref[...], normed, (((1,), (1,)), ((), ())), preferred_element_type=F32
        )
        for ref in (groups_ref, experts_ref)
    )
    routes = own_routes(tp_ref, routes_ref, normed.shape[0])
    group_size = expert_logits.shape[0] // group_logits.shape[0]
    groups = lax.broadcasted_iota(jnp.int32, group_logits.shape, 0)
    experts = lax.broadcasted_iota(jnp.int32, expert_logits.shape, 0)
    chosen = routes[0:1, :] // group_size
    own = jnp.sum(jnp.where(groups == chosen, group_logits, 0.0), axis=0, keepdims=True)
    share = 1.0 / jnp.sum(jnp.exp(group_logits - own), axis=0, keepdims=True)
    picked = [
        jnp.sum(jnp.where(experts == routes[k : k + 1, :], expert_logits, 0.0), axis=0, keepdims=True)
        for k in range(2)
    ]
    for k in range(2):
        out_ref[k : k + 1, :] = share / (1.0 + jnp.exp(picked[1 - k] - picked[k]))


def route_gates(tp, normed, group_router, expert_router, routes_t):
    (out,) = call(
        gates_kernel,
        (normed, group_router.T, expert_router.T, routes_t),
        (jax.ShapeDtypeStruct((2, normed.shape[0]), F32),),
        scalars=(tp,),
    )
    return out


def pack_weights_kernel(gate_ref, up_ref, down_ref, top_ref, bottom_ref):
    rows, lanes = gate_ref.shape
    extra = top_ref.shape[0] - rows
    top_ref[:rows, :] = gate_ref[...]
    top_ref[rows:, :] = up_ref[:extra, :]
    bottom_ref[: rows - extra, :] = up_ref[extra:, :]
    at = rows - extra
    for n in range(down_ref.shape[1] // lanes):
        bottom_ref[at : at + lanes, :] = down_ref[:, n * lanes : (n + 1) * lanes]
        at += lanes


def pack_weights(gate, up, down):
    rows, lanes = gate.shape
    shape = jax.ShapeDtypeStruct((3 * rows // 2, lanes), BF16)
    return windowed(pack_weights_kernel, (gate, up, down), (shape, shape), ())


def ffn_kernel(*refs, parts):
    sources, (rows_ref, out_ref, tops, bottoms, acc, sems) = refs[: 2 * parts], refs[2 * parts :]
    model = rows_ref.shape[1]
    lanes = tops.shape[2]
    extra = tops.shape[1] - model
    copies = []
    for n in range(parts):
        for k, (source, held) in enumerate(((sources[n], tops), (sources[parts + n], bottoms))):
            copies.append(pltpu.make_async_copy(source, held.at[n], sems.at[2 * n + k]))
    for copy in copies:
        copy.start()
    rows = rows_ref[...]
    for first in range(0, parts, 2):
        for copy in copies[2 * first : 2 * first + 4]:
            copy.wait()
        pair = (first, first + 1)
        gate = jnp.concatenate([tops[p, :model, :] for p in pair], axis=1)
        up = jnp.concatenate(
            [
                jnp.concatenate([tops[p, model:, :], bottoms[p, : model - extra, :]], axis=0)
                for p in pair
            ],
            axis=1,
        )
        g = jnp.dot(rows, gate, preferred_element_type=F32)
        u = jnp.dot(rows, up, preferred_element_type=F32)
        hidden = (g / (1.0 + jnp.exp(-g)) * u).astype(BF16)
        for n in range(0, model // lanes, 2):
            at = model - extra + n * lanes
            block = jnp.concatenate(
                [
                    jnp.concatenate(
                        [bottoms[p, at : at + lanes, :], bottoms[p, at + lanes : at + 2 * lanes, :]],
                        axis=1,
                    )
                    for p in pair
                ],
                axis=0,
            )
            part = jnp.dot(hidden, block, preferred_element_type=F32)
            to = slice(n * lanes, (n + 2) * lanes)
            if first:
                part += acc[:, to]
            if first + 2 < parts:
                acc[:, to] = part
            else:
                out_ref[:, to] = part.astype(BF16)


def ffn(rows, tops, bottoms):
    parts = len(tops)
    (out,) = call(
        functools.partial(ffn_kernel, parts=parts),
        (rows,),
        (jax.ShapeDtypeStruct(rows.shape, BF16),),
        streamed=(*tops, *bottoms),
        scratch=(
            pltpu.VMEM((parts, *tops[0].shape), BF16),
            pltpu.VMEM((parts, *bottoms[0].shape), BF16),
            pltpu.VMEM(rows.shape, F32),
            pltpu.SemaphoreType.DMA((2 * parts,)),
        ),
        vmem=WIDE,
    )
    return out


def pack_heads_kernel(where_ref, q_ref, k_ref, v_ref, kept_ref, sent_ref, q0_ref, q1_ref):
    _, half, two_depth = kept_ref.shape
    depth = two_depth // 2
    heads = q_ref.shape[1] // depth
    core = where_ref[2]
    for ref, side in ((kept_ref, core), (sent_ref, 1 - core)):
        rows = pl.ds(pl.multiple_of(side * half, half), half)
        for h in range(heads):
            at = slice(h * depth, (h + 1) * depth)
            for copy in range(2):
                ref[2 * h + copy, :, :depth] = k_ref[rows, at]
                ref[2 * h + copy, :, depth:] = v_ref[rows, at]
    late = jnp.where(where_ref[0] >= 4, 1, 0)
    for n, ref in enumerate((q0_ref, q1_ref)):
        h = n + late * (1 - 2 * n)
        ref[...] = q_ref[:, pl.ds(pl.multiple_of(h * depth, depth), depth)]


def query_pairs(n, back=False):
    pairs = []
    for z in range(8):
        for c in range(2):
            j = n if z < 4 else 1 - n
            u = min(z, 7 - z)
            here, there = 2 * z + c, 2 * (2 * (2 * c + j) + u // 2) + u % 2
            pairs.append((there, here) if back else (here, there))
    return pairs


COLUMN_OFFSETS = (0, -1, 1, 2)


def attend_kernel(where_ref, own_ref, other_ref, q0_ref, q1_ref, *refs, columns, scale):
    blocks, (gain_ref, out0_ref, out1_ref, acc, top_ref) = refs[:8], refs[8:]
    z, x, core = where_ref[0], where_ref[1], where_ref[2]
    slices, half, two_depth = blocks[0].shape
    depth = two_depth // 2
    width = depth // 2
    rows = q0_ref.shape[0]
    head = lax.rem(z // 2, 2)
    weight = jnp.where(z // 4 == core, own_ref[head], other_ref[head])
    u = 2 * lax.rem(z, 2) + core

    def folded(a, join):
        return functools.reduce(join, [a[:, n : n + depth] for n in range(0, a.shape[1], depth)])

    def fold(q, number, diagonal):
        block = jnp.concatenate([b[number] for b in blocks], axis=0)
        v = block[:, depth:]
        if diagonal:
            lane = lax.broadcasted_iota(jnp.int32, (rows, half), 1)
            row = lax.broadcasted_iota(jnp.int32, (rows, half), 0) + x * 2 * half
            allowed = []
            for offset in COLUMN_OFFSETS:
                column = lax.rem(x + offset + columns, columns)
                for side in (core, 1 - core):
                    allowed.append(lane + (column * 2 * half + side * half) <= row)
            allowed = jnp.concatenate(allowed, axis=1)
        for m in range(2):
            s = lax.dot_general(
                q[:, m * width : (m + 1) * width],
                block[:, m * width : (m + 1) * width],
                (((1,), (1,)), ((), ())),
                preferred_element_type=F32,
            )
            if diagonal:
                s = jnp.where(allowed, s, masked_score)
            top = jnp.max(folded(s, jnp.maximum), axis=1, keepdims=True)
            if not diagonal:
                old = top_ref[m, :, :1]
                top = jnp.maximum(top, old)
                keep = jnp.exp2((old - top) * scale)
            e = jnp.exp2((s - top) * scale)
            total = folded(e, jnp.add)
            mixed = jnp.dot(e.astype(BF16), v, preferred_element_type=F32)
            if not diagonal:
                mixed = mixed + acc[m, :, :depth] * keep
                total = total + acc[m, :, depth:] * keep
            acc[m, :, :depth] = mixed
            acc[m, :, depth:] = total
            top_ref[m] = jnp.broadcast_to(top, top_ref.shape[1:])

    def one_slice(n, carry):
        q = jnp.where(n == 0, q0_ref[...], q1_ref[...])
        mine = jnp.where(n == head, u, slices - 1 - u)
        fold(q, mine, True)

        def earlier(k, c):
            fold(q, k, False)
            return c

        lax.fori_loop(0, mine, earlier, 0)
        first, second = (
            acc[m, :, :depth] / jnp.sum(acc[m, :, depth:], axis=1, keepdims=True) for m in range(2)
        )
        out = first - weight * second
        out = out * lax.rsqrt(jnp.mean(out * out, axis=1, keepdims=True) + norm_eps)
        out = (out * gain_ref[...]).astype(BF16)
        for chosen, ref in ((0, out0_ref), (1, out1_ref)):

            @pl.when(n == chosen)
            def _(ref=ref):
                ref[...] = out

        return carry

    lax.fori_loop(0, 2, one_slice, 0)


def attend(where, queries, blocks, weights, head_gain, columns, scale):
    rows, depth = queries[0].shape
    out = jax.ShapeDtypeStruct((rows, depth), BF16)
    return call(
        functools.partial(attend_kernel, columns=columns, scale=scale),
        (*queries, *blocks, head_gain.reshape(1, depth)),
        (out, out),
        scalars=(where, *weights),
        scratch=(pltpu.VMEM((2, rows, 2 * depth), F32), pltpu.VMEM((2, rows, depth), F32)),
        vmem=16 * 1024 * 1024,
    )


def local(
    queries,
    keys,
    values,
    lambdas,
    head_gain,
    moe_input,
    ffn_gain,
    group_router,
    expert_router,
    routes,
    w_gate,
    w_up,
    w_down,
):
    z, x, _, core = (lax.axis_index(a) for a in EP_TP)
    tp = lax.axis_index(TP).reshape(1)
    where = jnp.stack([z, x, core])

    top, bottom = pack_weights(w_gate[0], w_up[0], w_down[0])
    top_f = shifted(top, "y", 1)
    bottom_b = shifted(bottom, "y", -1)
    bottom_f = shifted(bottom, "y", 1)
    top_b = shifted(top, "y", -1)
    top_o = shifted(top_f, "y", 1)
    bottom_o = shifted(bottom_b, "y", -1)

    rows = queries.shape[0]
    half = rows // 2
    depth = head_gain.shape[0]
    heads_here = lambdas.shape[0]
    columns = lax.axis_size("x")
    scale = math.log2(math.e) * (depth // 2) ** (-0.5)
    side = jax.ShapeDtypeStruct((2 * heads_here, half, 2 * depth), BF16)
    one_head = jax.ShapeDtypeStruct((rows, depth), BF16)
    kept, sent, q0, q1 = windowed(
        pack_heads_kernel, (queries, keys, values), (side, side, one_head, one_head), (where,)
    )
    got = shifted(sent, "c", 1)
    in_turn = []
    for n, q in enumerate((q0, q1)):
        in_turn.append(lax.ppermute(q, ("z", "c"), query_pairs(n)))
    spread = jnp.where(
        core == 0, jnp.concatenate([kept, got], axis=0), jnp.concatenate([got, kept], axis=0)
    )
    kv = lax.all_to_all(
        spread, "z", split_axis=0, concat_axis=0, tiled=True
    )
    kv_f, kv_b = shifted(kv, "x", 1), shifted(kv, "x", -1)
    kv_o = shifted(kv_f, "x", 1)
    blocks = []
    for block in (kv, kv_f, kv_b, kv_o):
        blocks += [block, shifted(block, "c", 1)]
    weights = (lambdas, shifted(lambdas, "c", 1))

    own_count = routes.shape[0] // lax.axis_size(TP)
    experts = expert_router.shape[1]
    capacity = 2 * own_count // experts
    model_width = moe_input.shape[1]
    routes_t = routes.T
    normed, packed = dispatch(tp, moe_input, ffn_gain, routes_t, own_count, experts, capacity)
    gates_t = route_gates(tp, normed, group_router, expert_router, routes_t)
    arrived = lax.all_to_all(
        packed.reshape(experts, capacity, model_width), EP, split_axis=0, concat_axis=0, tiled=True
    ).reshape(experts * capacity, model_width)
    tops, bottoms = [], []
    for t, b in ((top, bottom), (top_f, bottom_f), (top_b, bottom_b), (top_o, bottom_o)):
        tops += [t, shifted(t, "c", 1)]
        bottoms += [b, shifted(b, "c", 1)]
    results = ffn(arrived, tops, bottoms)
    homed = lax.all_to_all(
        results.reshape(experts, capacity, model_width), EP, split_axis=0, concat_axis=0, tiled=True
    ).reshape(experts * capacity, model_width)

    outgoing = attend(where, in_turn, blocks, weights, head_gain, columns, scale)
    incoming = []
    for n, m in enumerate(outgoing):
        incoming.append(lax.ppermute(m, ("z", "c"), query_pairs(n, back=True)))
    attn_out = jnp.where(
        z < 4, jnp.concatenate(incoming, axis=1), jnp.concatenate(incoming[::-1], axis=1)
    )

    moe_out = combine(tp, homed, gates_t, routes_t, own_count, experts, capacity)
    return (attn_out, moe_out)


def solution(mesh):
    split = Mesh(mesh.devices.reshape(8, 4, 4, 2), EP_TP)
    placed = (
        P(EP, TP),
        P(EP, TP),
        P(EP, TP),
        P(TP),
        P(),
        P(EP, None),
        P(),
        P(),
        P(),
        P(EP, None),
        P(EP, None, TP),
        P(EP, None, TP),
        P(EP, TP, None),
    )

    return jax.shard_map(
        local, mesh=split, in_specs=placed, out_specs=(P(EP, TP), P(EP_TP, None)), check_vma=False
    )
```

time: 317 us -> 181 us (0.57)
  the two profiles are of different devices: /device:TPU:238 before, /device:TPU:97 now
where the time goes in v2:
time: 181 us
  starting transfers between devices  73.9 us (41%)
  waiting for transfers between devices  70.5 us (39%)
  Pallas kernels  31.3 us (17%)
  other arithmetic  3.24 us (2%)
    ppermute x23, waiting for transfers between devices, shifted(): return lax.ppermute(array, axis, [(i, (i + by) % n) for i in range(n)])  58.2 us
    ppermute x23, starting transfers between devices, shifted(): return lax.ppermute(array, axis, [(i, (i + by) % n) for i in range(n)])  31.9 us
    pallas_call x4, Pallas kernels, call(): pl.pallas_call(body, in_specs=[pl.BlockSpec(memory_space=pltpu.SMEM)] * l...  23.4 us
    ppermute x2, starting transfers between devices, local(): incoming.append(lax.ppermute(m, ('z', 'c'), query_pairs(n, back=True)))  9.79 us
    all_to_all x1, starting transfers between devices, local(): lax.all_to_all(packed.reshape(experts, capacity, model_width), EP, split_...  9.72 us
    all_to_all x1, starting transfers between devices, local(): lax.all_to_all(results.reshape(experts, capacity, model_width), EP, split...  9.35 us
    pallas_call x3, Pallas kernels, windowed(): pl.pallas_call(body, grid_spec=pltpu.PrefetchScalarGridSpec(num_scalar_pr...  7.85 us
    ppermute x2, waiting for transfers between devices, local(): incoming.append(lax.ppermute(m, ('z', 'c'), query_pairs(n, back=True)))  7 us
  transfers between devices with their start and end apart: 30, of which 13 were waited for; matrix products, arithmetic and copies ran while one was open for 2% of the time, Pallas kernels for 15%

profile of v2, /device:TPU:97, one launch (start us, length us, event | category | flops | bytes accessed | tf_op | source)
XLA Modules:
  0.0 180.7 jit_solution(9136642884192815510)
XLA Ops:
  0.6 2.7 %shard_map.143 = (bf16[128,2048]{1,0:T(8,128)(2,1)}, bf16[256,2048]{1,0:T(8,128)(2,1)}) custom-call(s32[1]{0:T(128)} %bitcast.4.tp_ref, bf16[1024,2048]{1,0:T(8,128)(2,1)} %rows_ref.1, f32[1,2048]{1,0:T(1,128)} %bitcast.29, s32[2,1024]{1,0:T(2,128)} %bitcast.18), custom_call_target="tpu_custom_call" | custom-call | tf_op jit(solution)/shard_map/pallas_call | solution.py:33
  3.4 9.7 %all-to-all-start.1 = ((bf16[32,8,2048]{2,1,0:T(8,128)(2,1)}), bf16[32,8,2048]{2,1,0:T(8,128)(2,1)S(1)}, u32[]{:S(2)}, u32[]{:S(2)}) async-start(bf16[32,8,2048]{2,1,0:T(8,128)(2,1)} %bitcast.25), calls=%async_computation.1 | async-start | bytes 2097152 | tf_op jit(solution)/shard_map/all_to_all | solution.py:440
  13.1 2.6 %shard_map.142 = (bf16[3072,128]{1,0:T(8,128)(2,1)}, bf16[3072,128]{1,0:T(8,128)(2,1)}) custom-call(bf16[2048,128]{1,0:T(8,128)(2,1)} %bitcast.26, bf16[2048,128]{1,0:T(8,128)(2,1)} %bitcast.27, bf16[128,2048]{1,0:T(8,128)(2,1)} %bitcast.28), custom_call_target="tpu_custom_call" | custom-call | tf_op jit(solution)/shard_map/pallas_call | solution.py:33
  15.7 2.7 %collective-permute-start.16 = (bf16[3072,128]{1,0:T(8,128)(2,1)}, bf16[3072,128]{1,0:T(8,128)(2,1)S(1)}, u32[]{:S(2)}, u32[]{:S(2)}) collective-permute-start(bf16[3072,128]{1,0:T(8,128)(2,1)} %get-tuple-element.18.refs_0_), channel_id=1, source_target_pairs={{0,6},{2,0},{4,2},{6,4},{1,7},{3,1},{5,3},{7,5},{8,14},{10,8},{12,... | collective-permute-start | bytes 2359304 | tf_op jit(solution)/shard_map/ppermute | solution.py:26
  19.9 3.0 %collective-permute-start.23 = (bf16[3072,128]{1,0:T(8,128)(2,1)}, bf16[3072,128]{1,0:T(8,128)(2,1)}, u32[]{:S(2)}, u32[]{:S(2)}) collective-permute-start(bf16[3072,128]{1,0:T(8,128)(2,1)} %get-tuple-element.19.refs_8_), channel_id=1, source_target_pairs={{0,6},{2,0},{4,2},{6,4},{1,7},{3,1},{5,3},{7,5},{8,14},{10,8},{12,... | collective-permute-start | bytes 2359304 | tf_op jit(solution)/shard_map/ppermute | solution.py:26
  23.5 2.6 %shard_map.140 = (bf16[4,128,256]{2,1,0:T(8,128)(2,1)}, bf16[4,128,256]{2,1,0:T(8,128)(2,1)}, bf16[256,128]{1,0:T(8,128)(2,1)}, bf16[256,128]{1,0:T(8,128)(2,1)}) custom-call(s32[3]{0:T(128)} %pad_add_fusion.where_ref, bf16[256,256]{1,0:T(8,128)(2,1)} %q_ref.1, bf16[256,256]{1,0:T(8,128)(2,1)} %k_ref.1, bf16[256,256]{1,0:T(8,128)(2,1)} %v_ref.1), custom_call_target="tpu_custom_call" | custom-call | tf_op jit(solution)/shard_map/pallas_call | solution.py:33
  27.8 6.6 %collective-permute-done.16.refs_4_ = bf16[3072,128]{1,0:T(8,128)(2,1)S(1)} collective-permute-done((bf16[3072,128]{1,0:T(8,128)(2,1)}, bf16[3072,128]{1,0:T(8,128)(2,1)S(1)}, u32[]{:S(2)}, u32[]{:S(2)}) %collective-permute-start.16) | collective-permute-done | bytes 786464 | tf_op jit(solution)/shard_map/ppermute | solution.py:26
  34.4 3.8 %collective-permute-start.20 = (bf16[3072,128]{1,0:T(8,128)(2,1)}, bf16[3072,128]{1,0:T(8,128)(2,1)}, u32[]{:S(2)}, u32[]{:S(2)}) collective-permute-start(bf16[3072,128]{1,0:T(8,128)(2,1)} %get-tuple-element.19.refs_8_), channel_id=1, source_target_pairs={{0,1},{1,0},{2,3},{3,2},{4,5},{5,4},{6,7},{7,6},{8,9},{9,8},{10,11... | collective-permute-start | bytes 2359304 | tf_op jit(solution)/shard_map/ppermute | solution.py:26
  38.2 3.6 %collective-permute-start.17 = (bf16[3072,128]{1,0:T(8,128)(2,1)S(1)}, bf16[3072,128]{1,0:T(8,128)(2,1)}, u32[]{:S(2)}, u32[]{:S(2)}) collective-permute-start(bf16[3072,128]{1,0:T(8,128)(2,1)S(1)} %collective-permute-done.16.refs_4_), channel_id=1, source_target_pairs={{0,1},{1,0},{2,3},{3,2},{4,5},{5,4},{6,7},{7,6},{8,9},{9,8},{10,11... | collective-permute-start | bytes 2359304 | tf_op jit(solution)/shard_map/ppermute | solution.py:26
  41.7 9.5 %collective-permute-done.23.refs_12_ = bf16[3072,128]{1,0:T(8,128)(2,1)} collective-permute-done((bf16[3072,128]{1,0:T(8,128)(2,1)}, bf16[3072,128]{1,0:T(8,128)(2,1)}, u32[]{:S(2)}, u32[]{:S(2)}) %collective-permute-start.23) | collective-permute-done | bytes 786464 | tf_op jit(solution)/shard_map/ppermute | solution.py:26
  51.2 3.4 %collective-permute-start.25 = (bf16[3072,128]{1,0:T(8,128)(2,1)}, bf16[3072,128]{1,0:T(8,128)(2,1)}, u32[]{:S(2)}, u32[]{:S(2)}) collective-permute-start(bf16[3072,128]{1,0:T(8,128)(2,1)} %collective-permute-done.23.refs_12_), channel_id=1, source_target_pairs={{0,6},{2,0},{4,2},{6,4},{1,7},{3,1},{5,3},{7,5},{8,14},{10,8},{12,... | collective-permute-start | bytes 2359304 | tf_op jit(solution)/shard_map/ppermute | solution.py:26
  56.5 6.6 %all-to-all-start = ((bf16[8,128,256]{2,1,0:T(8,128)(2,1)}), bf16[8,128,256]{2,1,0:T(8,128)(2,1)S(1)}, u32[]{:S(2)}, u32[]{:S(2)}) async-start(bf16[8,128,256]{2,1,0:T(8,128)(2,1)} %maximum_select_fusion), calls=%async_computation | async-start | bytes 1048576 | tf_op jit(solution)/shard_map/all_to_all | solution.py:423
  63.2 2.9 %collective-permute-start.15 = (bf16[3072,128]{1,0:T(8,128)(2,1)S(1)}, bf16[3072,128]{1,0:T(8,128)(2,1)S(1)}, u32[]{:S(2)}, u32[]{:S(2)}) collective-permute-start(bf16[3072,128]{1,0:T(8,128)(2,1)S(1)} %collective-permute-done.14.refs_2_), channel_id=1, source_target_pairs={{0,1},{1,0},{2,3},{3,2},{4,5},{5,4},{6,7},{7,6},{8,9},{9,8},{10,11... | collective-permute-start | bytes 2359304 | tf_op jit(solution)/shard_map/ppermute | solution.py:26
  66.6 4.6 %collective-permute-done.18.refs_6_ = bf16[3072,128]{1,0:T(8,128)(2,1)} collective-permute-done((bf16[3072,128]{1,0:T(8,128)(2,1)S(1)}, bf16[3072,128]{1,0:T(8,128)(2,1)}, u32[]{:S(2)}, u32[]{:S(2)}) %collective-permute-start.18) | collective-permute-done | bytes 786464 | tf_op jit(solution)/shard_map/ppermute | solution.py:26
  71.2 2.4 %collective-permute-start.19 = (bf16[3072,128]{1,0:T(8,128)(2,1)}, bf16[3072,128]{1,0:T(8,128)(2,1)S(1)}, u32[]{:S(2)}, u32[]{:S(2)}) collective-permute-start(bf16[3072,128]{1,0:T(8,128)(2,1)} %collective-permute-done.18.refs_6_), channel_id=1, source_target_pairs={{0,1},{1,0},{2,3},{3,2},{4,5},{5,4},{6,7},{7,6},{8,9},{9,8},{10,11... | collective-permute-start | bytes 2359304 | tf_op jit(solution)/shard_map/ppermute | solution.py:26
  77.7 8.5 %shard_map.144 = bf16[256,2048]{1,0:T(8,128)(2,1)} custom-call(bf16[3072,128]{1,0:T(8,128)(2,1)} %get-tuple-element.18.refs_0_, bf16[3072,128]{1,0:T(8,128)(2,1)} %collective-permute-done.13.refs_1_, bf16[3072,128]{1,0:T(8,128)(2,1)} %copy-done.9, bf16[3072,128]{1,0:T(8,128)(2,1)} %copy-done.10, bf16[3072,128]{1,0:T(8,128)(2,1)} %copy-done.8, ...), custom_call_target="tpu_custom_call" | custom-call | tf_op jit(solution)/shard_map/pallas_call | solution.py:47
  86.3 9.3 %all-to-all-start.2 = ((bf16[32,8,2048]{2,1,0:T(8,128)(2,1)}), bf16[32,8,2048]{2,1,0:T(8,128)(2,1)S(1)}, u32[]{:S(2)}, u32[]{:S(2)}) async-start(bf16[32,8,2048]{2,1,0:T(8,128)(2,1)} %bitcast.24), calls=%async_computation.2 | async-start | bytes 2097152 | tf_op jit(solution)/shard_map/all_to_all | solution.py:448
  98.4 20.8 %collective-permute-done.5.refs_2_ = bf16[8,128,256]{2,1,0:T(8,128)(2,1)S(1)} collective-permute-done((bf16[8,128,256]{2,1,0:T(8,128)(2,1)S(1)}, bf16[8,128,256]{2,1,0:T(8,128)(2,1)S(1)}, u32[]{:S(2)}, u32[]{:S(2)}) %collective-permute-start.5) | collective-permute-done | bytes 524320 | tf_op jit(solution)/shard_map/ppermute | solution.py:26
  122.1 10.6 %collective-permute-done.9.refs_6_ = bf16[8,128,256]{2,1,0:T(8,128)(2,1)S(1)} collective-permute-done((bf16[8,128,256]{2,1,0:T(8,128)(2,1)S(1)}, bf16[8,128,256]{2,1,0:T(8,128)(2,1)S(1)}, u32[]{:S(2)}, u32[]{:S(2)}) %collective-permute-start.9) | collective-permute-done | bytes 524320 | tf_op jit(solution)/shard_map/ppermute | solution.py:26
  136.4 4.6 %collective-permute-start.1 = (bf16[256,128]{1,0:T(8,128)(2,1)S(1)}, bf16[256,128]{1,0:T(8,128)(2,1)S(1)}, u32[]{:S(2)}, u32[]{:S(2)}) collective-permute-start(bf16[256,128]{1,0:T(8,128)(2,1)S(1)} %copy-done.16), channel_id=1, source_target_pairs={{0,0},{1,128},{32,1},{33,129},{64,32},{65,160},{96,33},{97,161},{1... | collective-permute-start | bytes 196616 | tf_op jit(solution)/shard_map/ppermute | solution.py:419
  141.1 3.9 %collective-permute-done.1.q0_ref = bf16[256,128]{1,0:T(8,128)(2,1)S(1)} collective-permute-done((bf16[256,128]{1,0:T(8,128)(2,1)S(1)}, bf16[256,128]{1,0:T(8,128)(2,1)S(1)}, u32[]{:S(2)}, u32[]{:S(2)}) %collective-permute-start.1) | collective-permute-done | bytes 65568 | tf_op jit(solution)/shard_map/ppermute | solution.py:419
  148.2 13.1 %shard_map.141 = (bf16[256,128]{1,0:T(8,128)(2,1)S(1)}, bf16[256,128]{1,0:T(8,128)(2,1)S(1)}) custom-call(s32[3]{0:T(128)S(1)} %copy-done.4, f32[2]{0:T(128)S(1)} %copy-done.5, f32[2]{0:T(128)S(1)} %collective-permute-done.other_ref, bf16[256,128]{1,0:T(8,128)(2,1)S(1)} %collective-permute-done.1.q0_ref, bf16[256,128]{1,0:T(8,128)(2,1)S(1)} %collective-permute-done.2.q1_ref, ...), custom_call_target="tpu_custom_call" | custom-call | tf_op jit(solution)/shard_map/pallas_call | solution.py:47
  161.3 9.7 %collective-permute-start.11 = (bf16[256,128]{1,0:T(8,128)(2,1)S(1)}, bf16[256,128]{1,0:T(8,128)(2,1)S(1)}, u32[]{:S(2)}, u32[]{:S(2)}) collective-permute-start(bf16[256,128]{1,0:T(8,128)(2,1)S(1)} %get-tuple-element.16), channel_id=1, source_target_pairs={{0,0},{128,1},{1,32},{129,33},{32,64},{160,65},{33,96},{161,97},{9... | collective-permute-start | bytes 196616 | tf_op jit(solution)/shard_map/ppermute | solution.py:455
  172.3 6.3 %collective-permute-done.12 = bf16[256,128]{1,0:T(8,128)(2,1)S(1)} collective-permute-done((bf16[256,128]{1,0:T(8,128)(2,1)S(1)}, bf16[256,128]{1,0:T(8,128)(2,1)S(1)}, u32[]{:S(2)}, u32[]{:S(2)}) %collective-permute-start.12) | collective-permute-done | bytes 65568 | tf_op jit(solution)/shard_map/ppermute | solution.py:455
  (80 shorter events, 26.4 us)
Async XLA Ops:
  3.4 53.2 %all-to-all-start.1 = ((bf16[32,8,2048]{2,1,0:T(8,128)(2,1)}), bf16[32,8,2048]{2,1,0:T(8,128)(2,1)S(1)}, u32[]{:S(2)}, u32[]{:S(2)}) async-start(bf16[32,8,2048]{2,1,0:T(8,128)(2,1)} %bitcast.25), calls=%async_computation.1 | async-start | bytes 2097152 | tf_op jit(solution)/shard_map/all_to_all | solution.py:440
  15.7 18.7 %collective-permute-start.16 = (bf16[3072,128]{1,0:T(8,128)(2,1)}, bf16[3072,128]{1,0:T(8,128)(2,1)S(1)}, u32[]{:S(2)}, u32[]{:S(2)}) collective-permute-start(bf16[3072,128]{1,0:T(8,128)(2,1)} %get-tuple-element.18.refs_0_), channel_id=1, source_target_pairs={{0,6},{2,0},{4,2},{6,4},{1,7},{3,1},{5,3},{7,5},{8,14},{10,8},{12,... | collective-permute-start | bytes 2359304 | tf_op jit(solution)/shard_map/ppermute | solution.py:26
  18.4 19.8 %collective-permute-start.14 = (bf16[3072,128]{1,0:T(8,128)(2,1)}, bf16[3072,128]{1,0:T(8,128)(2,1)S(1)}, u32[]{:S(2)}, u32[]{:S(2)}) collective-permute-start(bf16[3072,128]{1,0:T(8,128)(2,1)} %get-tuple-element.18.refs_0_), channel_id=1, source_target_pairs={{0,2},{2,4},{4,6},{6,0},{1,3},{3,5},{5,7},{7,1},{8,10},{10,12},{12... | collective-permute-start | bytes 2359304 | tf_op jit(solution)/shard_map/ppermute | solution.py:26
  18.4 23.3 %collective-permute-start.13 = (bf16[3072,128]{1,0:T(8,128)(2,1)}, bf16[3072,128]{1,0:T(8,128)(2,1)}, u32[]{:S(2)}, u32[]{:S(2)}) collective-permute-start(bf16[3072,128]{1,0:T(8,128)(2,1)} %get-tuple-element.18.refs_0_), channel_id=1, source_target_pairs={{0,1},{1,0},{2,3},{3,2},{4,5},{5,4},{6,7},{7,6},{8,9},{9,8},{10,11... | collective-permute-start | bytes 2359304 | tf_op jit(solution)/shard_map/ppermute | solution.py:26
  19.9 31.3 %collective-permute-start.23 = (bf16[3072,128]{1,0:T(8,128)(2,1)}, bf16[3072,128]{1,0:T(8,128)(2,1)}, u32[]{:S(2)}, u32[]{:S(2)}) collective-permute-start(bf16[3072,128]{1,0:T(8,128)(2,1)} %get-tuple-element.19.refs_8_), channel_id=1, source_target_pairs={{0,6},{2,0},{4,2},{6,4},{1,7},{3,1},{5,3},{7,5},{8,14},{10,8},{12,... | collective-permute-start | bytes 2359304 | tf_op jit(solution)/shard_map/ppermute | solution.py:26
  27.8 35.4 %collective-permute-start.21 = (bf16[3072,128]{1,0:T(8,128)(2,1)}, bf16[3072,128]{1,0:T(8,128)(2,1)}, u32[]{:S(2)}, u32[]{:S(2)}) collective-permute-start(bf16[3072,128]{1,0:T(8,128)(2,1)} %get-tuple-element.19.refs_8_), channel_id=1, source_target_pairs={{0,2},{2,4},{4,6},{6,0},{1,3},{3,5},{5,7},{7,1},{8,10},{10,12},{12... | collective-permute-start | bytes 2359304 | tf_op jit(solution)/shard_map/ppermute | solution.py:26
  34.4 31.8 %collective-permute-start.20 = (bf16[3072,128]{1,0:T(8,128)(2,1)}, bf16[3072,128]{1,0:T(8,128)(2,1)}, u32[]{:S(2)}, u32[]{:S(2)}) collective-permute-start(bf16[3072,128]{1,0:T(8,128)(2,1)} %get-tuple-element.19.refs_8_), channel_id=1, source_target_pairs={{0,1},{1,0},{2,3},{3,2},{4,5},{5,4},{6,7},{7,6},{8,9},{9,8},{10,11... | collective-permute-start | bytes 2359304 | tf_op jit(solution)/shard_map/ppermute | solution.py:26
  38.2 28.1 %collective-permute-start.17 = (bf16[3072,128]{1,0:T(8,128)(2,1)S(1)}, bf16[3072,128]{1,0:T(8,128)(2,1)}, u32[]{:S(2)}, u32[]{:S(2)}) collective-permute-start(bf16[3072,128]{1,0:T(8,128)(2,1)S(1)} %collective-permute-done.16.refs_4_), channel_id=1, source_target_pairs={{0,1},{1,0},{2,3},{3,2},{4,5},{5,4},{6,7},{7,6},{8,9},{9,8},{10,11... | collective-permute-start | bytes 2359304 | tf_op jit(solution)/shard_map/ppermute | solution.py:26
  41.7 29.5 %collective-permute-start.18 = (bf16[3072,128]{1,0:T(8,128)(2,1)S(1)}, bf16[3072,128]{1,0:T(8,128)(2,1)}, u32[]{:S(2)}, u32[]{:S(2)}) collective-permute-start(bf16[3072,128]{1,0:T(8,128)(2,1)S(1)} %collective-permute-done.14.refs_2_), channel_id=1, source_target_pairs={{0,2},{2,4},{4,6},{6,0},{1,3},{3,5},{5,7},{7,1},{8,10},{10,12},{12... | collective-permute-start | bytes 2359304 | tf_op jit(solution)/shard_map/ppermute | solution.py:26
  51.2 22.4 %collective-permute-start.25 = (bf16[3072,128]{1,0:T(8,128)(2,1)}, bf16[3072,128]{1,0:T(8,128)(2,1)}, u32[]{:S(2)}, u32[]{:S(2)}) collective-permute-start(bf16[3072,128]{1,0:T(8,128)(2,1)} %collective-permute-done.23.refs_12_), channel_id=1, source_target_pairs={{0,6},{2,0},{4,2},{6,4},{1,7},{3,1},{5,3},{7,5},{8,14},{10,8},{12,... | collective-permute-start | bytes 2359304 | tf_op jit(solution)/shard_map/ppermute | solution.py:26
  56.5 29.7 %all-to-all-start = ((bf16[8,128,256]{2,1,0:T(8,128)(2,1)}), bf16[8,128,256]{2,1,0:T(8,128)(2,1)S(1)}, u32[]{:S(2)}, u32[]{:S(2)}) async-start(bf16[8,128,256]{2,1,0:T(8,128)(2,1)} %maximum_select_fusion), calls=%async_computation | async-start | bytes 1048576 | tf_op jit(solution)/shard_map/all_to_all | solution.py:423
  63.2 10.4 %collective-permute-start.15 = (bf16[3072,128]{1,0:T(8,128)(2,1)S(1)}, bf16[3072,128]{1,0:T(8,128)(2,1)S(1)}, u32[]{:S(2)}, u32[]{:S(2)}) collective-permute-start(bf16[3072,128]{1,0:T(8,128)(2,1)S(1)} %collective-permute-done.14.refs_2_), channel_id=1, source_target_pairs={{0,1},{1,0},{2,3},{3,2},{4,5},{5,4},{6,7},{7,6},{8,9},{9,8},{10,11... | collective-permute-start | bytes 2359304 | tf_op jit(solution)/shard_map/ppermute | solution.py:26
  66.1 7.5 %collective-permute-start.24 = (bf16[3072,128]{1,0:T(8,128)(2,1)}, bf16[3072,128]{1,0:T(8,128)(2,1)S(1)}, u32[]{:S(2)}, u32[]{:S(2)}) collective-permute-start(bf16[3072,128]{1,0:T(8,128)(2,1)} %collective-permute-done.23.refs_12_), channel_id=1, source_target_pairs={{0,1},{1,0},{2,3},{3,2},{4,5},{5,4},{6,7},{7,6},{8,9},{9,8},{10,11... | collective-permute-start | bytes 2359304 | tf_op jit(solution)/shard_map/ppermute | solution.py:26
  86.3 92.9 %all-to-all-start.2 = ((bf16[32,8,2048]{2,1,0:T(8,128)(2,1)}), bf16[32,8,2048]{2,1,0:T(8,128)(2,1)S(1)}, u32[]{:S(2)}, u32[]{:S(2)}) async-start(bf16[32,8,2048]{2,1,0:T(8,128)(2,1)} %bitcast.24), calls=%async_computation.2 | async-start | bytes 2097152 | tf_op jit(solution)/shard_map/all_to_all | solution.py:448
  95.7 23.5 %collective-permute-start.5 = (bf16[8,128,256]{2,1,0:T(8,128)(2,1)S(1)}, bf16[8,128,256]{2,1,0:T(8,128)(2,1)S(1)}, u32[]{:S(2)}, u32[]{:S(2)}) collective-permute-start(bf16[8,128,256]{2,1,0:T(8,128)(2,1)S(1)} %all-to-all-done.refs_0_), channel_id=1, source_target_pairs={{0,8},{8,16},{16,24},{24,0},{1,9},{9,17},{17,25},{25,1},{2,10},{10... | collective-permute-start | bytes 1572872 | tf_op jit(solution)/shard_map/ppermute | solution.py:26
  96.9 24.7 %collective-permute-start.7 = (bf16[8,128,256]{2,1,0:T(8,128)(2,1)S(1)}, bf16[8,128,256]{2,1,0:T(8,128)(2,1)S(1)}, u32[]{:S(2)}, u32[]{:S(2)}) collective-permute-start(bf16[8,128,256]{2,1,0:T(8,128)(2,1)S(1)} %all-to-all-done.refs_0_), channel_id=1, source_target_pairs={{0,24},{8,0},{16,8},{24,16},{1,25},{9,1},{17,9},{25,17},{2,26},{10... | collective-permute-start | bytes 1572872 | tf_op jit(solution)/shard_map/ppermute | solution.py:26
  119.2 13.6 %collective-permute-start.9 = (bf16[8,128,256]{2,1,0:T(8,128)(2,1)S(1)}, bf16[8,128,256]{2,1,0:T(8,128)(2,1)S(1)}, u32[]{:S(2)}, u32[]{:S(2)}) collective-permute-start(bf16[8,128,256]{2,1,0:T(8,128)(2,1)S(1)} %collective-permute-done.5.refs_2_), channel_id=1, source_target_pairs={{0,8},{8,16},{16,24},{24,0},{1,9},{9,17},{17,25},{25,1},{2,10},{10... | collective-permute-start | bytes 1572872 | tf_op jit(solution)/shard_map/ppermute | solution.py:26
  120.2 28.0 %collective-permute-start.4 = (bf16[8,128,256]{2,1,0:T(8,128)(2,1)S(1)}, bf16[8,128,256]{2,1,0:T(8,128)(2,1)S(1)}, u32[]{:S(2)}, u32[]{:S(2)}) collective-permute-start(bf16[8,128,256]{2,1,0:T(8,128)(2,1)S(1)} %all-to-all-done.refs_0_), channel_id=1, source_target_pairs={{0,1},{1,0},{2,3},{3,2},{4,5},{5,4},{6,7},{7,6},{8,9},{9,8},{10,11... | collective-permute-start | bytes 1572872 | tf_op jit(solution)/shard_map/ppermute | solution.py:26
  121.6 26.5 %collective-permute-start.6 = (bf16[8,128,256]{2,1,0:T(8,128)(2,1)S(1)}, bf16[8,128,256]{2,1,0:T(8,128)(2,1)S(1)}, u32[]{:S(2)}, u32[]{:S(2)}) collective-permute-start(bf16[8,128,256]{2,1,0:T(8,128)(2,1)S(1)} %collective-permute-done.5.refs_2_), channel_id=1, source_target_pairs={{0,1},{1,0},{2,3},{3,2},{4,5},{5,4},{6,7},{7,6},{8,9},{9,8},{10,11... | collective-permute-start | bytes 1572872 | tf_op jit(solution)/shard_map/ppermute | solution.py:26
  121.6 26.5 %collective-permute-start.8 = (bf16[8,128,256]{2,1,0:T(8,128)(2,1)S(1)}, bf16[8,128,256]{2,1,0:T(8,128)(2,1)S(1)}, u32[]{:S(2)}, u32[]{:S(2)}) collective-permute-start(bf16[8,128,256]{2,1,0:T(8,128)(2,1)S(1)} %collective-permute-done.7.refs_4_), channel_id=1, source_target_pairs={{0,1},{1,0},{2,3},{3,2},{4,5},{5,4},{6,7},{7,6},{8,9},{9,8},{10,11... | collective-permute-start | bytes 1572872 | tf_op jit(solution)/shard_map/ppermute | solution.py:26
  132.8 15.4 %collective-permute-start.10 = (bf16[8,128,256]{2,1,0:T(8,128)(2,1)S(1)}, bf16[8,128,256]{2,1,0:T(8,128)(2,1)S(1)}, u32[]{:S(2)}, u32[]{:S(2)}) collective-permute-start(bf16[8,128,256]{2,1,0:T(8,128)(2,1)S(1)} %collective-permute-done.9.refs_6_), channel_id=1, source_target_pairs={{0,1},{1,0},{2,3},{3,2},{4,5},{5,4},{6,7},{7,6},{8,9},{9,8},{10,11... | collective-permute-start | bytes 1572872 | tf_op jit(solution)/shard_map/ppermute | solution.py:26
  136.4 8.6 %collective-permute-start.1 = (bf16[256,128]{1,0:T(8,128)(2,1)S(1)}, bf16[256,128]{1,0:T(8,128)(2,1)S(1)}, u32[]{:S(2)}, u32[]{:S(2)}) collective-permute-start(bf16[256,128]{1,0:T(8,128)(2,1)S(1)} %copy-done.16), channel_id=1, source_target_pairs={{0,0},{1,128},{32,1},{33,129},{64,32},{65,160},{96,33},{97,161},{1... | collective-permute-start | bytes 196616 | tf_op jit(solution)/shard_map/ppermute | solution.py:419
  161.3 11.0 %collective-permute-start.11 = (bf16[256,128]{1,0:T(8,128)(2,1)S(1)}, bf16[256,128]{1,0:T(8,128)(2,1)S(1)}, u32[]{:S(2)}, u32[]{:S(2)}) collective-permute-start(bf16[256,128]{1,0:T(8,128)(2,1)S(1)} %get-tuple-element.16), channel_id=1, source_target_pairs={{0,0},{128,1},{1,32},{129,33},{32,64},{160,65},{33,96},{161,97},{9... | collective-permute-start | bytes 196616 | tf_op jit(solution)/shard_map/ppermute | solution.py:455
  171.0 7.6 %collective-permute-start.12 = (bf16[256,128]{1,0:T(8,128)(2,1)S(1)}, bf16[256,128]{1,0:T(8,128)(2,1)S(1)}, u32[]{:S(2)}, u32[]{:S(2)}) collective-permute-start(bf16[256,128]{1,0:T(8,128)(2,1)S(1)} %get-tuple-element.17), channel_id=1, source_target_pairs={{64,0},{192,1},{65,32},{193,33},{96,64},{224,65},{97,96},{225,97},... | collective-permute-start | bytes 196616 | tf_op jit(solution)/shard_map/ppermute | solution.py:455
  (23 other events, 798.3 us)

commit v3 on v2

--- a/solution.py
+++ b/solution.py
@@ -186,8 +186,8 @@
     return windowed(pack_weights_kernel, (gate, up, down), (shape, shape), ())
 
 
-def ffn_kernel(*refs, parts):
-    sources, (rows_ref, out_ref, tops, bottoms, acc, sems) = refs[: 2 * parts], refs[2 * parts :]
+def ffn_kernel(rows_in, *refs, parts):
+    sources, (out_ref, rows_ref, tops, bottoms, acc, sems) = refs[: 2 * parts], refs[2 * parts :]
     model = rows_ref.shape[1]
     lanes = tops.shape[2]
     extra = tops.shape[1] - model
@@ -195,12 +195,17 @@
     for n in range(parts):
         for k, (source, held) in enumerate(((sources[n], tops), (sources[parts + n], bottoms))):
             copies.append(pltpu.make_async_copy(source, held.at[n], sems.at[2 * n + k]))
-    for copy in copies:
+    rows_copy = pltpu.make_async_copy(rows_in, rows_ref, sems.at[2 * parts])
+    rows_copy.start()
+    for copy in copies[:8]:
         copy.start()
+    rows_copy.wait()
     rows = rows_ref[...]
     for first in range(0, parts, 2):
         for copy in copies[2 * first : 2 * first + 4]:
             copy.wait()
+        for copy in copies[2 * first + 8 : 2 * first + 12]:
+            copy.start()
         pair = (first, first + 1)
         gate = jnp.concatenate([tops[p, :model, :] for p in pair], axis=1)
         up = jnp.concatenate(
@@ -239,25 +244,26 @@
     parts = len(tops)
     (out,) = call(
         functools.partial(ffn_kernel, parts=parts),
-        (rows,),
+        (),
         (jax.ShapeDtypeStruct(rows.shape, BF16),),
-        streamed=(*tops, *bottoms),
+        streamed=(rows, *tops, *bottoms),
         scratch=(
+            pltpu.VMEM(rows.shape, BF16),
             pltpu.VMEM((parts, *tops[0].shape), BF16),
             pltpu.VMEM((parts, *bottoms[0].shape), BF16),
             pltpu.VMEM(rows.shape, F32),
-            pltpu.SemaphoreType.DMA((2 * parts,)),
+            pltpu.SemaphoreType.DMA((2 * parts + 1,)),
         ),
-        vmem=WIDE,
+        vmem=56 * 1024 * 1024,
     )
     return out
 
 
-def pack_heads_kernel(where_ref, q_ref, k_ref, v_ref, kept_ref, sent_ref, q0_ref, q1_ref):
+def pack_heads_kernel(q_ref, k_ref, v_ref, kept_ref, sent_ref, q0_ref, q1_ref):
     _, half, two_depth = kept_ref.shape
     depth = two_depth // 2
     heads = q_ref.shape[1] // depth
-    core = where_ref[2]
+    core = lax.axis_index("c")
     for ref, side in ((kept_ref, core), (sent_ref, 1 - core)):
         rows = pl.ds(pl.multiple_of(side * half, half), half)
         for h in range(heads):
@@ -265,7 +271,7 @@
             for copy in range(2):
                 ref[2 * h + copy, :, :depth] = k_ref[rows, at]
                 ref[2 * h + copy, :, depth:] = v_ref[rows, at]
-    late = jnp.where(where_ref[0] >= 4, 1, 0)
+    late = jnp.where(lax.axis_index("z") >= 4, 1, 0)
     for n, ref in enumerate((q0_ref, q1_ref)):
         h = n + late * (1 - 2 * n)
         ref[...] = q_ref[:, pl.ds(pl.multiple_of(h * depth, depth), depth)]
@@ -285,9 +291,9 @@
 COLUMN_OFFSETS = (0, -1, 1, 2)
 
 
-def attend_kernel(where_ref, own_ref, other_ref, q0_ref, q1_ref, *refs, columns, scale):
+def attend_kernel(own_ref, other_ref, q0_ref, q1_ref, *refs, columns, scale):
     blocks, (gain_ref, out0_ref, out1_ref, acc, top_ref) = refs[:8], refs[8:]
-    z, x, core = where_ref[0], where_ref[1], where_ref[2]
+    z, x, core = (lax.axis_index(a) for a in ("z", "x", "c"))
     slices, half, two_depth = blocks[0].shape
     depth = two_depth // 2
     width = depth // 2
@@ -362,14 +368,14 @@
     lax.fori_loop(0, 2, one_slice, 0)
 
 
-def attend(where, queries, blocks, weights, head_gain, columns, scale):
+def attend(queries, blocks, weights, head_gain, columns, scale):
     rows, depth = queries[0].shape
     out = jax.ShapeDtypeStruct((rows, depth), BF16)
     return call(
         functools.partial(attend_kernel, columns=columns, scale=scale),
         (*queries, *blocks, head_gain.reshape(1, depth)),
         (out, out),
-        scalars=(where, *weights),
+        scalars=weights,
         scratch=(pltpu.VMEM((2, rows, 2 * depth), F32), pltpu.VMEM((2, rows, depth), F32)),
         vmem=16 * 1024 * 1024,
     )
@@ -390,9 +396,8 @@
     w_up,
     w_down,
 ):
-    z, x, _, core = (lax.axis_index(a) for a in EP_TP)
+    z, _, _, core = (lax.axis_index(a) for a in EP_TP)
     tp = lax.axis_index(TP).reshape(1)
-    where = jnp.stack([z, x, core])
 
     top, bottom = pack_weights(w_gate[0], w_up[0], w_down[0])
     top_f = shifted(top, "y", 1)
@@ -411,7 +416,7 @@
     side = jax.ShapeDtypeStruct((2 * heads_here, half, 2 * depth), BF16)
     one_head = jax.ShapeDtypeStruct((rows, depth), BF16)
     kept, sent, q0, q1 = windowed(
-        pack_heads_kernel, (queries, keys, values), (side, side, one_head, one_head), (where,)
+        pack_heads_kernel, (queries, keys, values), (side, side, one_head, one_head), ()
     )
     got = shifted(sent, "c", 1)
     in_turn = []
@@ -449,7 +454,7 @@
         results.reshape(experts, capacity, model_width), EP, split_axis=0, concat_axis=0, tiled=True
     ).reshape(experts * capacity, model_width)
 
-    outgoing = attend(where, in_turn, blocks, weights, head_gain, columns, scale)
+    outgoing = attend(in_turn, blocks, weights, head_gain, columns, scale)
     incoming = []
     for n, m in enumerate(outgoing):
         incoming.append(lax.ppermute(m, ("z", "c"), query_pairs(n, back=True)))

time: 181 us -> 180 us (level)
  transfers between devices with their start and end apart: 30 -> 30, of which waited for: 13 -> 13; matrix products, arithmetic and copies ran while one was open for 2% -> 1% of each run, Pallas kernels for 15% -> 14%
where the time goes in v3:
time: 180 us
  starting transfers between devices  73.9 us (41%)
  waiting for transfers between devices  71.8 us (40%)
  Pallas kernels  29.7 us (16%)
  other arithmetic  2.6 us (1%)
    ppermute x23, waiting for transfers between devices, shifted(): return lax.ppermute(array, axis, [(i, (i + by) % n) for i in range(n)])  59.5 us
    ppermute x23, starting transfers between devices, shifted(): return lax.ppermute(array, axis, [(i, (i + by) % n) for i in range(n)])  31.9 us
    pallas_call x4, Pallas kernels, call(): pl.pallas_call(body, in_specs=[pl.BlockSpec(memory_space=pltpu.SMEM)] * l...  22.5 us
    ppermute x2, starting transfers between devices, local(): incoming.append(lax.ppermute(m, ('z', 'c'), query_pairs(n, back=True)))  9.78 us
    all_to_all x1, starting transfers between devices, local(): lax.all_to_all(packed.reshape(experts, capacity, model_width), EP, split_...  9.72 us
    all_to_all x1, starting transfers between devices, local(): lax.all_to_all(results.reshape(experts, capacity, model_width), EP, split...  9.35 us
    pallas_call x3, Pallas kernels, windowed(): pl.pallas_call(body, grid_spec=pltpu.PrefetchScalarGridSpec(num_scalar_pr...  7.22 us
    ppermute x2, waiting for transfers between devices, local(): incoming.append(lax.ppermute(m, ('z', 'c'), query_pairs(n, back=True)))  7.01 us
  transfers between devices with their start and end apart: 30, of which 13 were waited for; matrix products, arithmetic and copies ran while one was open for 1% of the time, Pallas kernels for 14%

profile of v3, /device:TPU:97, one launch (start us, length us, event | category | flops | bytes accessed | tf_op | source)
XLA Modules:
  0.0 179.8 jit_solution(3856993905710014703)
XLA Ops:
  0.6 2.7 %shard_map.142 = (bf16[128,2048]{1,0:T(8,128)(2,1)}, bf16[256,2048]{1,0:T(8,128)(2,1)}) custom-call(s32[1]{0:T(128)} %bitcast.1.tp_ref, bf16[1024,2048]{1,0:T(8,128)(2,1)} %rows_ref.1, f32[1,2048]{1,0:T(1,128)} %bitcast.26, s32[2,1024]{1,0:T(2,128)} %bitcast.15), custom_call_target="tpu_custom_call" | custom-call | tf_op jit(solution)/shard_map/pallas_call | solution.py:33
  3.4 9.7 %all-to-all-start.1 = ((bf16[32,8,2048]{2,1,0:T(8,128)(2,1)}), bf16[32,8,2048]{2,1,0:T(8,128)(2,1)S(1)}, u32[]{:S(2)}, u32[]{:S(2)}) async-start(bf16[32,8,2048]{2,1,0:T(8,128)(2,1)} %bitcast.22), calls=%async_computation.1 | async-start | bytes 2097152 | tf_op jit(solution)/shard_map/all_to_all | solution.py:445
  13.1 2.6 %shard_map.143 = (bf16[3072,128]{1,0:T(8,128)(2,1)}, bf16[3072,128]{1,0:T(8,128)(2,1)}) custom-call(bf16[2048,128]{1,0:T(8,128)(2,1)} %bitcast.23, bf16[2048,128]{1,0:T(8,128)(2,1)} %bitcast.24, bf16[128,2048]{1,0:T(8,128)(2,1)} %bitcast.25), custom_call_target="tpu_custom_call" | custom-call | tf_op jit(solution)/shard_map/pallas_call | solution.py:33
  15.7 2.7 %collective-permute-start.16 = (bf16[3072,128]{1,0:T(8,128)(2,1)}, bf16[3072,128]{1,0:T(8,128)(2,1)S(1)}, u32[]{:S(2)}, u32[]{:S(2)}) collective-permute-start(bf16[3072,128]{1,0:T(8,128)(2,1)} %get-tuple-element.19.refs_0_), channel_id=1, source_target_pairs={{0,6},{2,0},{4,2},{6,4},{1,7},{3,1},{5,3},{7,5},{8,14},{10,8},{12,... | collective-permute-start | bytes 2359304 | tf_op jit(solution)/shard_map/ppermute | solution.py:26
  19.9 3.0 %collective-permute-start.23 = (bf16[3072,128]{1,0:T(8,128)(2,1)}, bf16[3072,128]{1,0:T(8,128)(2,1)}, u32[]{:S(2)}, u32[]{:S(2)}) collective-permute-start(bf16[3072,128]{1,0:T(8,128)(2,1)} %get-tuple-element.20.refs_8_), channel_id=1, source_target_pairs={{0,6},{2,0},{4,2},{6,4},{1,7},{3,1},{5,3},{7,5},{8,14},{10,8},{12,... | collective-permute-start | bytes 2359304 | tf_op jit(solution)/shard_map/ppermute | solution.py:26
  26.5 7.8 %collective-permute-done.16.refs_4_ = bf16[3072,128]{1,0:T(8,128)(2,1)S(1)} collective-permute-done((bf16[3072,128]{1,0:T(8,128)(2,1)}, bf16[3072,128]{1,0:T(8,128)(2,1)S(1)}, u32[]{:S(2)}, u32[]{:S(2)}) %collective-permute-start.16) | collective-permute-done | bytes 786464 | tf_op jit(solution)/shard_map/ppermute | solution.py:26
  34.4 3.8 %collective-permute-start.20 = (bf16[3072,128]{1,0:T(8,128)(2,1)}, bf16[3072,128]{1,0:T(8,128)(2,1)}, u32[]{:S(2)}, u32[]{:S(2)}) collective-permute-start(bf16[3072,128]{1,0:T(8,128)(2,1)} %get-tuple-element.20.refs_8_), channel_id=1, source_target_pairs={{0,1},{1,0},{2,3},{3,2},{4,5},{5,4},{6,7},{7,6},{8,9},{9,8},{10,11... | collective-permute-start | bytes 2359304 | tf_op jit(solution)/shard_map/ppermute | solution.py:26
  38.2 3.6 %collective-permute-start.17 = (bf16[3072,128]{1,0:T(8,128)(2,1)S(1)}, bf16[3072,128]{1,0:T(8,128)(2,1)}, u32[]{:S(2)}, u32[]{:S(2)}) collective-permute-start(bf16[3072,128]{1,0:T(8,128)(2,1)S(1)} %collective-permute-done.16.refs_4_), channel_id=1, source_target_pairs={{0,1},{1,0},{2,3},{3,2},{4,5},{5,4},{6,7},{7,6},{8,9},{9,8},{10,11... | collective-permute-start | bytes 2359304 | tf_op jit(solution)/shard_map/ppermute | solution.py:26
  41.8 9.5 %collective-permute-done.23.refs_12_ = bf16[3072,128]{1,0:T(8,128)(2,1)} collective-permute-done((bf16[3072,128]{1,0:T(8,128)(2,1)}, bf16[3072,128]{1,0:T(8,128)(2,1)}, u32[]{:S(2)}, u32[]{:S(2)}) %collective-permute-start.23) | collective-permute-done | bytes 786464 | tf_op jit(solution)/shard_map/ppermute | solution.py:26
  51.2 3.4 %collective-permute-start.25 = (bf16[3072,128]{1,0:T(8,128)(2,1)}, bf16[3072,128]{1,0:T(8,128)(2,1)}, u32[]{:S(2)}, u32[]{:S(2)}) collective-permute-start(bf16[3072,128]{1,0:T(8,128)(2,1)} %collective-permute-done.23.refs_12_), channel_id=1, source_target_pairs={{0,6},{2,0},{4,2},{6,4},{1,7},{3,1},{5,3},{7,5},{8,14},{10,8},{12,... | collective-permute-start | bytes 2359304 | tf_op jit(solution)/shard_map/ppermute | solution.py:26
  56.6 6.6 %all-to-all-start = ((bf16[8,128,256]{2,1,0:T(8,128)(2,1)}), bf16[8,128,256]{2,1,0:T(8,128)(2,1)S(1)}, u32[]{:S(2)}, u32[]{:S(2)}) async-start(bf16[8,128,256]{2,1,0:T(8,128)(2,1)} %maximum_select_fusion), calls=%async_computation | async-start | bytes 1048576 | tf_op jit(solution)/shard_map/all_to_all | solution.py:428
  63.2 2.9 %collective-permute-start.15 = (bf16[3072,128]{1,0:T(8,128)(2,1)S(1)}, bf16[3072,128]{1,0:T(8,128)(2,1)S(1)}, u32[]{:S(2)}, u32[]{:S(2)}) collective-permute-start(bf16[3072,128]{1,0:T(8,128)(2,1)S(1)} %collective-permute-done.14.refs_2_), channel_id=1, source_target_pairs={{0,1},{1,0},{2,3},{3,2},{4,5},{5,4},{6,7},{7,6},{8,9},{9,8},{10,11... | collective-permute-start | bytes 2359304 | tf_op jit(solution)/shard_map/ppermute | solution.py:26
  66.7 4.6 %collective-permute-done.18.refs_6_ = bf16[3072,128]{1,0:T(8,128)(2,1)} collective-permute-done((bf16[3072,128]{1,0:T(8,128)(2,1)S(1)}, bf16[3072,128]{1,0:T(8,128)(2,1)}, u32[]{:S(2)}, u32[]{:S(2)}) %collective-permute-start.18) | collective-permute-done | bytes 786464 | tf_op jit(solution)/shard_map/ppermute | solution.py:26
  71.2 2.4 %collective-permute-start.19 = (bf16[3072,128]{1,0:T(8,128)(2,1)}, bf16[3072,128]{1,0:T(8,128)(2,1)S(1)}, u32[]{:S(2)}, u32[]{:S(2)}) collective-permute-start(bf16[3072,128]{1,0:T(8,128)(2,1)} %collective-permute-done.18.refs_6_), channel_id=1, source_target_pairs={{0,1},{1,0},{2,3},{3,2},{4,5},{5,4},{6,7},{7,6},{8,9},{9,8},{10,11... | collective-permute-start | bytes 2359304 | tf_op jit(solution)/shard_map/ppermute | solution.py:26
  77.7 7.6 %shard_map.144 = bf16[256,2048]{1,0:T(8,128)(2,1)} custom-call(bf16[256,2048]{1,0:T(8,128)(2,1)} %bitcast.21, bf16[3072,128]{1,0:T(8,128)(2,1)} %get-tuple-element.19.refs_0_, bf16[3072,128]{1,0:T(8,128)(2,1)} %collective-permute-done.13.refs_1_, bf16[3072,128]{1,0:T(8,128)(2,1)} %copy-done.8, bf16[3072,128]{1,0:T(8,128)(2,1)} %copy-done.9, ...), custom_call_target="tpu_custom_call" | custom-call | tf_op jit(solution)/shard_map/pallas_call | solution.py:47
  85.4 9.4 %all-to-all-start.2 = ((bf16[32,8,2048]{2,1,0:T(8,128)(2,1)}), bf16[32,8,2048]{2,1,0:T(8,128)(2,1)S(1)}, u32[]{:S(2)}, u32[]{:S(2)}) async-start(bf16[32,8,2048]{2,1,0:T(8,128)(2,1)} %bitcast.20), calls=%async_computation.2 | async-start | bytes 2097152 | tf_op jit(solution)/shard_map/all_to_all | solution.py:453
  97.5 20.8 %collective-permute-done.5.refs_2_ = bf16[8,128,256]{2,1,0:T(8,128)(2,1)S(1)} collective-permute-done((bf16[8,128,256]{2,1,0:T(8,128)(2,1)S(1)}, bf16[8,128,256]{2,1,0:T(8,128)(2,1)S(1)}, u32[]{:S(2)}, u32[]{:S(2)}) %collective-permute-start.5) | collective-permute-done | bytes 524320 | tf_op jit(solution)/shard_map/ppermute | solution.py:26
  121.2 10.6 %collective-permute-done.9.refs_6_ = bf16[8,128,256]{2,1,0:T(8,128)(2,1)S(1)} collective-permute-done((bf16[8,128,256]{2,1,0:T(8,128)(2,1)S(1)}, bf16[8,128,256]{2,1,0:T(8,128)(2,1)S(1)}, u32[]{:S(2)}, u32[]{:S(2)}) %collective-permute-start.9) | collective-permute-done | bytes 524320 | tf_op jit(solution)/shard_map/ppermute | solution.py:26
  131.9 2.1 %collective-permute-start.10 = (bf16[8,128,256]{2,1,0:T(8,128)(2,1)S(1)}, bf16[8,128,256]{2,1,0:T(8,128)(2,1)S(1)}, u32[]{:S(2)}, u32[]{:S(2)}) collective-permute-start(bf16[8,128,256]{2,1,0:T(8,128)(2,1)S(1)} %collective-permute-done.9.refs_6_), channel_id=1, source_target_pairs={{0,1},{1,0},{2,3},{3,2},{4,5},{5,4},{6,7},{7,6},{8,9},{9,8},{10,11... | collective-permute-start | bytes 1572872 | tf_op jit(solution)/shard_map/ppermute | solution.py:26
  135.5 4.6 %collective-permute-start.1 = (bf16[256,128]{1,0:T(8,128)(2,1)S(1)}, bf16[256,128]{1,0:T(8,128)(2,1)S(1)}, u32[]{:S(2)}, u32[]{:S(2)}) collective-permute-start(bf16[256,128]{1,0:T(8,128)(2,1)S(1)} %copy-done.15), channel_id=1, source_target_pairs={{0,0},{1,128},{32,1},{33,129},{64,32},{65,160},{96,33},{97,161},{1... | collective-permute-start | bytes 196616 | tf_op jit(solution)/shard_map/ppermute | solution.py:424
  140.2 3.9 %collective-permute-done.1.q0_ref = bf16[256,128]{1,0:T(8,128)(2,1)S(1)} collective-permute-done((bf16[256,128]{1,0:T(8,128)(2,1)S(1)}, bf16[256,128]{1,0:T(8,128)(2,1)S(1)}, u32[]{:S(2)}, u32[]{:S(2)}) %collective-permute-start.1) | collective-permute-done | bytes 65568 | tf_op jit(solution)/shard_map/ppermute | solution.py:424
  147.3 13.1 %shard_map.141 = (bf16[256,128]{1,0:T(8,128)(2,1)S(1)}, bf16[256,128]{1,0:T(8,128)(2,1)S(1)}) custom-call(f32[2]{0:T(128)S(1)} %copy-done.4, f32[2]{0:T(128)S(1)} %collective-permute-done.other_ref, bf16[256,128]{1,0:T(8,128)(2,1)S(1)} %collective-permute-done.1.q0_ref, bf16[256,128]{1,0:T(8,128)(2,1)S(1)} %collective-permute-done.2.q1_ref, ...), custom_call_target="tpu_custom_call" | custom-call | tf_op jit(solution)/shard_map/pallas_call | solution.py:47
  160.4 9.7 %collective-permute-start.11 = (bf16[256,128]{1,0:T(8,128)(2,1)S(1)}, bf16[256,128]{1,0:T(8,128)(2,1)S(1)}, u32[]{:S(2)}, u32[]{:S(2)}) collective-permute-start(bf16[256,128]{1,0:T(8,128)(2,1)S(1)} %get-tuple-element.16), channel_id=1, source_target_pairs={{0,0},{128,1},{1,32},{129,33},{32,64},{160,65},{33,96},{161,97},{9... | collective-permute-start | bytes 196616 | tf_op jit(solution)/shard_map/ppermute | solution.py:460
  171.4 6.3 %collective-permute-done.12 = bf16[256,128]{1,0:T(8,128)(2,1)S(1)} collective-permute-done((bf16[256,128]{1,0:T(8,128)(2,1)S(1)}, bf16[256,128]{1,0:T(8,128)(2,1)S(1)}, u32[]{:S(2)}, u32[]{:S(2)}) %collective-permute-start.12) | collective-permute-done | bytes 65568 | tf_op jit(solution)/shard_map/ppermute | solution.py:460
  (77 shorter events, 25.6 us)
Async XLA Ops:
  3.4 53.2 %all-to-all-start.1 = ((bf16[32,8,2048]{2,1,0:T(8,128)(2,1)}), bf16[32,8,2048]{2,1,0:T(8,128)(2,1)S(1)}, u32[]{:S(2)}, u32[]{:S(2)}) async-start(bf16[32,8,2048]{2,1,0:T(8,128)(2,1)} %bitcast.22), calls=%async_computation.1 | async-start | bytes 2097152 | tf_op jit(solution)/shard_map/all_to_all | solution.py:445
  15.7 18.7 %collective-permute-start.16 = (bf16[3072,128]{1,0:T(8,128)(2,1)}, bf16[3072,128]{1,0:T(8,128)(2,1)S(1)}, u32[]{:S(2)}, u32[]{:S(2)}) collective-permute-start(bf16[3072,128]{1,0:T(8,128)(2,1)} %get-tuple-element.19.refs_0_), channel_id=1, source_target_pairs={{0,6},{2,0},{4,2},{6,4},{1,7},{3,1},{5,3},{7,5},{8,14},{10,8},{12,... | collective-permute-start | bytes 2359304 | tf_op jit(solution)/shard_map/ppermute | solution.py:26
  18.4 19.8 %collective-permute-start.14 = (bf16[3072,128]{1,0:T(8,128)(2,1)}, bf16[3072,128]{1,0:T(8,128)(2,1)S(1)}, u32[]{:S(2)}, u32[]{:S(2)}) collective-permute-start(bf16[3072,128]{1,0:T(8,128)(2,1)} %get-tuple-element.19.refs_0_), channel_id=1, source_target_pairs={{0,2},{2,4},{4,6},{6,0},{1,3},{3,5},{5,7},{7,1},{8,10},{10,12},{12... | collective-permute-start | bytes 2359304 | tf_op jit(solution)/shard_map/ppermute | solution.py:26
  18.4 23.3 %collective-permute-start.13 = (bf16[3072,128]{1,0:T(8,128)(2,1)}, bf16[3072,128]{1,0:T(8,128)(2,1)}, u32[]{:S(2)}, u32[]{:S(2)}) collective-permute-start(bf16[3072,128]{1,0:T(8,128)(2,1)} %get-tuple-element.19.refs_0_), channel_id=1, source_target_pairs={{0,1},{1,0},{2,3},{3,2},{4,5},{5,4},{6,7},{7,6},{8,9},{9,8},{10,11... | collective-permute-start | bytes 2359304 | tf_op jit(solution)/shard_map/ppermute | solution.py:26
  19.9 31.3 %collective-permute-start.23 = (bf16[3072,128]{1,0:T(8,128)(2,1)}, bf16[3072,128]{1,0:T(8,128)(2,1)}, u32[]{:S(2)}, u32[]{:S(2)}) collective-permute-start(bf16[3072,128]{1,0:T(8,128)(2,1)} %get-tuple-element.20.refs_8_), channel_id=1, source_target_pairs={{0,6},{2,0},{4,2},{6,4},{1,7},{3,1},{5,3},{7,5},{8,14},{10,8},{12,... | collective-permute-start | bytes 2359304 | tf_op jit(solution)/shard_map/ppermute | solution.py:26
  26.5 36.7 %collective-permute-start.21 = (bf16[3072,128]{1,0:T(8,128)(2,1)}, bf16[3072,128]{1,0:T(8,128)(2,1)}, u32[]{:S(2)}, u32[]{:S(2)}) collective-permute-start(bf16[3072,128]{1,0:T(8,128)(2,1)} %get-tuple-element.20.refs_8_), channel_id=1, source_target_pairs={{0,2},{2,4},{4,6},{6,0},{1,3},{3,5},{5,7},{7,1},{8,10},{10,12},{12... | collective-permute-start | bytes 2359304 | tf_op jit(solution)/shard_map/ppermute | solution.py:26
  34.4 31.8 %collective-permute-start.20 = (bf16[3072,128]{1,0:T(8,128)(2,1)}, bf16[3072,128]{1,0:T(8,128)(2,1)}, u32[]{:S(2)}, u32[]{:S(2)}) collective-permute-start(bf16[3072,128]{1,0:T(8,128)(2,1)} %get-tuple-element.20.refs_8_), channel_id=1, source_target_pairs={{0,1},{1,0},{2,3},{3,2},{4,5},{5,4},{6,7},{7,6},{8,9},{9,8},{10,11... | collective-permute-start | bytes 2359304 | tf_op jit(solution)/shard_map/ppermute | solution.py:26
  38.2 28.1 %collective-permute-start.17 = (bf16[3072,128]{1,0:T(8,128)(2,1)S(1)}, bf16[3072,128]{1,0:T(8,128)(2,1)}, u32[]{:S(2)}, u32[]{:S(2)}) collective-permute-start(bf16[3072,128]{1,0:T(8,128)(2,1)S(1)} %collective-permute-done.16.refs_4_), channel_id=1, source_target_pairs={{0,1},{1,0},{2,3},{3,2},{4,5},{5,4},{6,7},{7,6},{8,9},{9,8},{10,11... | collective-permute-start | bytes 2359304 | tf_op jit(solution)/shard_map/ppermute | solution.py:26
  41.8 29.5 %collective-permute-start.18 = (bf16[3072,128]{1,0:T(8,128)(2,1)S(1)}, bf16[3072,128]{1,0:T(8,128)(2,1)}, u32[]{:S(2)}, u32[]{:S(2)}) collective-permute-start(bf16[3072,128]{1,0:T(8,128)(2,1)S(1)} %collective-permute-done.14.refs_2_), channel_id=1, source_target_pairs={{0,2},{2,4},{4,6},{6,0},{1,3},{3,5},{5,7},{7,1},{8,10},{10,12},{12... | collective-permute-start | bytes 2359304 | tf_op jit(solution)/shard_map/ppermute | solution.py:26
  51.2 22.4 %collective-permute-start.25 = (bf16[3072,128]{1,0:T(8,128)(2,1)}, bf16[3072,128]{1,0:T(8,128)(2,1)}, u32[]{:S(2)}, u32[]{:S(2)}) collective-permute-start(bf16[3072,128]{1,0:T(8,128)(2,1)} %collective-permute-done.23.refs_12_), channel_id=1, source_target_pairs={{0,6},{2,0},{4,2},{6,4},{1,7},{3,1},{5,3},{7,5},{8,14},{10,8},{12,... | collective-permute-start | bytes 2359304 | tf_op jit(solution)/shard_map/ppermute | solution.py:26
  56.6 28.8 %all-to-all-start = ((bf16[8,128,256]{2,1,0:T(8,128)(2,1)}), bf16[8,128,256]{2,1,0:T(8,128)(2,1)S(1)}, u32[]{:S(2)}, u32[]{:S(2)}) async-start(bf16[8,128,256]{2,1,0:T(8,128)(2,1)} %maximum_select_fusion), calls=%async_computation | async-start | bytes 1048576 | tf_op jit(solution)/shard_map/all_to_all | solution.py:428
  63.2 10.4 %collective-permute-start.15 = (bf16[3072,128]{1,0:T(8,128)(2,1)S(1)}, bf16[3072,128]{1,0:T(8,128)(2,1)S(1)}, u32[]{:S(2)}, u32[]{:S(2)}) collective-permute-start(bf16[3072,128]{1,0:T(8,128)(2,1)S(1)} %collective-permute-done.14.refs_2_), channel_id=1, source_target_pairs={{0,1},{1,0},{2,3},{3,2},{4,5},{5,4},{6,7},{7,6},{8,9},{9,8},{10,11... | collective-permute-start | bytes 2359304 | tf_op jit(solution)/shard_map/ppermute | solution.py:26
  66.1 7.5 %collective-permute-start.24 = (bf16[3072,128]{1,0:T(8,128)(2,1)}, bf16[3072,128]{1,0:T(8,128)(2,1)S(1)}, u32[]{:S(2)}, u32[]{:S(2)}) collective-permute-start(bf16[3072,128]{1,0:T(8,128)(2,1)} %collective-permute-done.23.refs_12_), channel_id=1, source_target_pairs={{0,1},{1,0},{2,3},{3,2},{4,5},{5,4},{6,7},{7,6},{8,9},{9,8},{10,11... | collective-permute-start | bytes 2359304 | tf_op jit(solution)/shard_map/ppermute | solution.py:26
  85.4 92.9 %all-to-all-start.2 = ((bf16[32,8,2048]{2,1,0:T(8,128)(2,1)}), bf16[32,8,2048]{2,1,0:T(8,128)(2,1)S(1)}, u32[]{:S(2)}, u32[]{:S(2)}) async-start(bf16[32,8,2048]{2,1,0:T(8,128)(2,1)} %bitcast.20), calls=%async_computation.2 | async-start | bytes 2097152 | tf_op jit(solution)/shard_map/all_to_all | solution.py:453
  94.8 23.5 %collective-permute-start.5 = (bf16[8,128,256]{2,1,0:T(8,128)(2,1)S(1)}, bf16[8,128,256]{2,1,0:T(8,128)(2,1)S(1)}, u32[]{:S(2)}, u32[]{:S(2)}) collective-permute-start(bf16[8,128,256]{2,1,0:T(8,128)(2,1)S(1)} %all-to-all-done.refs_0_), channel_id=1, source_target_pairs={{0,8},{8,16},{16,24},{24,0},{1,9},{9,17},{17,25},{25,1},{2,10},{10... | collective-permute-start | bytes 1572872 | tf_op jit(solution)/shard_map/ppermute | solution.py:26
  96.0 24.7 %collective-permute-start.7 = (bf16[8,128,256]{2,1,0:T(8,128)(2,1)S(1)}, bf16[8,128,256]{2,1,0:T(8,128)(2,1)S(1)}, u32[]{:S(2)}, u32[]{:S(2)}) collective-permute-start(bf16[8,128,256]{2,1,0:T(8,128)(2,1)S(1)} %all-to-all-done.refs_0_), channel_id=1, source_target_pairs={{0,24},{8,0},{16,8},{24,16},{1,25},{9,1},{17,9},{25,17},{2,26},{10... | collective-permute-start | bytes 1572872 | tf_op jit(solution)/shard_map/ppermute | solution.py:26
  118.3 13.6 %collective-permute-start.9 = (bf16[8,128,256]{2,1,0:T(8,128)(2,1)S(1)}, bf16[8,128,256]{2,1,0:T(8,128)(2,1)S(1)}, u32[]{:S(2)}, u32[]{:S(2)}) collective-permute-start(bf16[8,128,256]{2,1,0:T(8,128)(2,1)S(1)} %collective-permute-done.5.refs_2_), channel_id=1, source_target_pairs={{0,8},{8,16},{16,24},{24,0},{1,9},{9,17},{17,25},{25,1},{2,10},{10... | collective-permute-start | bytes 1572872 | tf_op jit(solution)/shard_map/ppermute | solution.py:26
  119.2 28.0 %collective-permute-start.4 = (bf16[8,128,256]{2,1,0:T(8,128)(2,1)S(1)}, bf16[8,128,256]{2,1,0:T(8,128)(2,1)S(1)}, u32[]{:S(2)}, u32[]{:S(2)}) collective-permute-start(bf16[8,128,256]{2,1,0:T(8,128)(2,1)S(1)} %all-to-all-done.refs_0_), channel_id=1, source_target_pairs={{0,1},{1,0},{2,3},{3,2},{4,5},{5,4},{6,7},{7,6},{8,9},{9,8},{10,11... | collective-permute-start | bytes 1572872 | tf_op jit(solution)/shard_map/ppermute | solution.py:26
  120.7 26.5 %collective-permute-start.6 = (bf16[8,128,256]{2,1,0:T(8,128)(2,1)S(1)}, bf16[8,128,256]{2,1,0:T(8,128)(2,1)S(1)}, u32[]{:S(2)}, u32[]{:S(2)}) collective-permute-start(bf16[8,128,256]{2,1,0:T(8,128)(2,1)S(1)} %collective-permute-done.5.refs_2_), channel_id=1, source_target_pairs={{0,1},{1,0},{2,3},{3,2},{4,5},{5,4},{6,7},{7,6},{8,9},{9,8},{10,11... | collective-permute-start | bytes 1572872 | tf_op jit(solution)/shard_map/ppermute | solution.py:26
  120.7 26.5 %collective-permute-start.8 = (bf16[8,128,256]{2,1,0:T(8,128)(2,1)S(1)}, bf16[8,128,256]{2,1,0:T(8,128)(2,1)S(1)}, u32[]{:S(2)}, u32[]{:S(2)}) collective-permute-start(bf16[8,128,256]{2,1,0:T(8,128)(2,1)S(1)} %collective-permute-done.7.refs_4_), channel_id=1, source_target_pairs={{0,1},{1,0},{2,3},{3,2},{4,5},{5,4},{6,7},{7,6},{8,9},{9,8},{10,11... | collective-permute-start | bytes 1572872 | tf_op jit(solution)/shard_map/ppermute | solution.py:26
  131.9 15.4 %collective-permute-start.10 = (bf16[8,128,256]{2,1,0:T(8,128)(2,1)S(1)}, bf16[8,128,256]{2,1,0:T(8,128)(2,1)S(1)}, u32[]{:S(2)}, u32[]{:S(2)}) collective-permute-start(bf16[8,128,256]{2,1,0:T(8,128)(2,1)S(1)} %collective-permute-done.9.refs_6_), channel_id=1, source_target_pairs={{0,1},{1,0},{2,3},{3,2},{4,5},{5,4},{6,7},{7,6},{8,9},{9,8},{10,11... | collective-permute-start | bytes 1572872 | tf_op jit(solution)/shard_map/ppermute | solution.py:26
  135.5 8.6 %collective-permute-start.1 = (bf16[256,128]{1,0:T(8,128)(2,1)S(1)}, bf16[256,128]{1,0:T(8,128)(2,1)S(1)}, u32[]{:S(2)}, u32[]{:S(2)}) collective-permute-start(bf16[256,128]{1,0:T(8,128)(2,1)S(1)} %copy-done.15), channel_id=1, source_target_pairs={{0,0},{1,128},{32,1},{33,129},{64,32},{65,160},{96,33},{97,161},{1... | collective-permute-start | bytes 196616 | tf_op jit(solution)/shard_map/ppermute | solution.py:424
  160.4 11.0 %collective-permute-start.11 = (bf16[256,128]{1,0:T(8,128)(2,1)S(1)}, bf16[256,128]{1,0:T(8,128)(2,1)S(1)}, u32[]{:S(2)}, u32[]{:S(2)}) collective-permute-start(bf16[256,128]{1,0:T(8,128)(2,1)S(1)} %get-tuple-element.16), channel_id=1, source_target_pairs={{0,0},{128,1},{1,32},{129,33},{32,64},{160,65},{33,96},{161,97},{9... | collective-permute-start | bytes 196616 | tf_op jit(solution)/shard_map/ppermute | solution.py:460
  170.1 7.6 %collective-permute-start.12 = (bf16[256,128]{1,0:T(8,128)(2,1)S(1)}, bf16[256,128]{1,0:T(8,128)(2,1)S(1)}, u32[]{:S(2)}, u32[]{:S(2)}) collective-permute-start(bf16[256,128]{1,0:T(8,128)(2,1)S(1)} %get-tuple-element.17), channel_id=1, source_target_pairs={{64,0},{192,1},{65,32},{193,33},{96,64},{224,65},{97,96},{225,97},... | collective-permute-start | bytes 196616 | tf_op jit(solution)/shard_map/ppermute | solution.py:460
  (22 other events, 724.1 us)
